TPU v7x, 128 devices: a whole 4x4x4 slice. The times are simulated.
128 devices in a mesh: sp: 16 (over z, y), dp: 8 (over x, core).
Axes of the slice: x: 4, y: 4, z: 4, core: 2. Of those that a mesh axis runs over, the one named last changes fastest.
Arguments:
- tokens: bfloat16 [8, 2048, 2048], P('dp', 'sp'), may hold values from -6 to 6
- cotangent: bfloat16 [8, 2048, 2048], P('dp', 'sp'), may hold values from -6 to 6
- value_weight: bfloat16 [2048, 2048], P(('sp', 'dp')), may hold values from -0.125 to 0.125
- query_heads: bfloat16 [8, 2048, 16, 128], P('dp', None, 'sp'), may hold values from -8 to 8
- key_heads: bfloat16 [8, 2048, 16, 128], P('dp', None, 'sp'), may hold values from -8 to 8
- lambdas: float32 [16], P('sp'), may hold values from 0.3 to 0.8
Outputs:
- grad_query: bfloat16 [8, 2048, 16, 128], P('dp', None, 'sp')
- grad_key: bfloat16 [8, 2048, 16, 128], P('dp', None, 'sp')
- grad_tokens: bfloat16 [8, 2048, 2048], P('dp', 'sp')
- grad_value_weight: float32 [2048, 2048], P(('sp', 'dp'))
- grad_lambda: float32 [16], P('sp')
All inputs are finite; a program needn't handle non-finite values.
Results may differ from a plain program's by a relative error of at most 0.0095.
Values may be sent and summed in bfloat16 or wider, within the bound.
A program may use at most 192 MiB of HBM per device.

v0:
```python
import functools, math
import jax, jax.numpy as jnp
from jax import lax
from jax.experimental import pallas as pl
from jax.experimental.pallas import tpu as pltpu
from jax.sharding import PartitionSpec as P

EPS = 1e-6
B = 256
NB = 8
SCALE = 0.125
LOG2E = 1.4426950408889634
F32 = jnp.float32
BF = jnp.bfloat16

def nt(a, b):
    return lax.dot_general(a, b, (((1,), (1,)), ((), ())), preferred_element_type=F32)

def nn(a, b):
    return lax.dot_general(a, b, (((1,), (0,)), ((), ())), preferred_element_type=F32)

def tri(i, j):
    return (i * (i + 1)) // 2 + j

def paired(lo, n, body):
    def two(p, c):
        body(lo + 2 * p, 2)
        return c
    lax.fori_loop(0, n // 2, two, 0)
    def one(p, c):
        body(lo + n - 1, 1)
        return c
    lax.fori_loop(0, n % 2, one, 0)

def prepare(i, q_ref, k_ref, qz1, qz2, kt):
    rows = pl.ds(pl.multiple_of(i * B, B), B)
    q = q_ref[rows, :]
    first = lax.broadcasted_iota(jnp.int32, (B, 128), 1) < 64
    zero = jnp.zeros_like(q)
    qz1[i] = jnp.where(first, q, zero)
    qz2[i] = jnp.where(first, zero, q)
    kt[i] = k_ref[rows, :].T

def softmaxes(i, lam, k_ref, qz1, qz2, s1, s2, p1, p2, aa):
    q1, q2 = qz1[i], qz2[i]

    def score(j, m):
        k = k_ref[pl.ds(pl.multiple_of(j * B, B), B), :]
        a, b = nt(k, q1), nt(k, q2)
        return a, b

    def keep(j, a, b, m):
        s1[j] = a
        s2[j] = b
        return (jnp.maximum(m[0], jnp.max(a.reshape(B // 8, 8, B), axis=0)),
                jnp.maximum(m[1], jnp.max(b.reshape(B // 8, 8, B), axis=0)))

    a, b = score(i, None)
    seen = lax.broadcasted_iota(jnp.int32, (B, B), 0) <= lax.broadcasted_iota(jnp.int32, (B, B), 1)
    a = jnp.where(seen, a, -1e30)
    b = jnp.where(seen, b, -1e30)
    low = jnp.full((8, B), -1e30, F32)
    m = keep(i, a, b, (low, low))

    def off(j, m):
        a, b = score(j, m)
        return keep(j, a, b, m)
    def two(p, m):
        a, b = score(2 * p, m)
        c, d = score(2 * p + 1, m)
        m = keep(2 * p, a, b, m)
        return keep(2 * p + 1, c, d, m)
    m = lax.fori_loop(0, i // 2, two, m)
    m = lax.fori_loop(i - i % 2, i, off, m)
    m1 = jnp.max(m[0], axis=0, keepdims=True)
    m2 = jnp.max(m[1], axis=0, keepdims=True)
    c = SCALE * LOG2E

    def power(j, l):
        e1 = jnp.exp2((s1[j] - m1) * c)
        e2 = jnp.exp2((s2[j] - m2) * c)
        s1[j] = e1
        s2[j] = e2
        return (l[0] + jnp.sum(e1.reshape(B // 8, 8, B), axis=0),
                l[1] + jnp.sum(e2.reshape(B // 8, 8, B), axis=0))
    l = lax.fori_loop(0, i + 1, power, (jnp.zeros((8, B), F32), jnp.zeros((8, B), F32)))
    r1 = 1.0 / jnp.sum(l[0], axis=0, keepdims=True)
    r2 = 1.0 / jnp.sum(l[1], axis=0, keepdims=True)

    def norm(j, _):
        x1 = s1[j] * r1
        x2 = s2[j] * r2
        t = tri(i, j)
        p1[t] = x1.astype(BF)
        p2[t] = x2.astype(BF)
        aa[t] = (x1 - lam * x2).astype(BF)
        return _
    lax.fori_loop(0, i + 1, norm, 0)

def mixed(i, lam, vt, p2, aa, cot_ref, dot, do, delta):
    def acc(j, c):
        t = tri(i, j)
        v = vt[j]
        return c[0] + nn(v, aa[t]), c[1] + nn(v, p2[t])
    zero = jnp.zeros((128, B), F32)
    o, o2 = lax.fori_loop(0, i + 1, acc, (zero, zero))
    g = cot_ref[pl.ds(pl.multiple_of(i * B, B), B), :].astype(F32).T
    r = lax.rsqrt(jnp.mean(o * o, axis=0, keepdims=True) + EPS)
    y = r * o
    d = (r * (g - y * jnp.mean(g * y, axis=0, keepdims=True))).astype(BF)
    dw = d.astype(F32)
    d2 = jnp.sum(dw * o2, axis=0, keepdims=True)
    d1 = jnp.sum(dw * o, axis=0, keepdims=True) + lam * d2
    dot[i] = d
    do[i] = dw.T.astype(BF)
    delta[i, 0:1, :] = d1
    delta[i, 1:2, :] = d2
    return d2

def keys_block(j, vn, qz1, qz2, kt, p1, p2, aa, dot, do, delta, dqt):
    v = vn[j]
    k1t, k2t = kt[j, 0:64, :], kt[j, 64:128, :]

    def parts(i):
        t = tri(i, j)
        da = nn(v, dot[i])
        x1 = (p1[t].astype(F32) * (da - delta[i, 0:1, :])).astype(BF)
        x2 = (p2[t].astype(F32) * (da - delta[i, 1:2, :])).astype(BF)
        dv = nn(aa[t], do[i])
        dk1 = nn(x1, qz1[i])
        dk2 = nn(x2, qz2[i])
        dqt[i, 0:64, :] += nn(k1t, x1)
        dqt[i, 64:128, :] += nn(k2t, x2)
        return dv, dk1 , dk2

    def two(p, c):
        a = parts(j + 2 * p)
        b = parts(j + 2 * p + 1)
        return tuple(x + (y + z) for x, y, z in zip(c, a, b))
    def one(p, c):
        a = parts(p)
        return tuple(x + y for x, y in zip(c, a))
    n = NB - j
    zero = jnp.zeros((B, 128), F32)
    c = lax.fori_loop(0, n // 2, two, (zero, zero, zero))
    c = lax.fori_loop(NB - n % 2, NB, one, c)
    return c[0], c[1], c[2]

V = pltpu.VMEM
S = jax.ShapeDtypeStruct


def first_kernel(lam_ref, q_ref, k_ref, p1, p2, aa, qz1, qz2, kt, s1, s2):
    lam = lam_ref[0]
    lax.fori_loop(0, NB, lambda i, c: (prepare(i, q_ref, k_ref, qz1, qz2, kt), c)[1], 0)
    lax.fori_loop(0, NB, lambda i, c: (softmaxes(i, lam, k_ref, qz1, qz2, s1, s2, p1, p2, aa), c)[1], 0)


def second_kernel(lam_ref, q_ref, k_ref, v_ref, cot_ref, p1, p2, aa, gq, gk, gv, gl, qz1, qz2, kt, vt, vn, dot, do, delta, dqt):
    lam = lam_ref[0]

    def prep(i, c):
        prepare(i, q_ref, k_ref, qz1, qz2, kt)
        v = v_ref[pl.ds(pl.multiple_of(i * B, B), B), :]
        vn[i] = v
        vt[i] = v.T
        dqt[i] = jnp.zeros((128, B), F32)
        return c
    lax.fori_loop(0, NB, prep, 0)
    t = lax.fori_loop(0, NB, lambda i, c: c + mixed(i, lam, vt, p2, aa, cot_ref, dot, do, delta), jnp.zeros((1, B), F32))
    gl[...] = jnp.broadcast_to(-jnp.sum(t, axis=1, keepdims=True), (8, 128))
    half = lax.broadcasted_iota(jnp.int32, (1, 128), 1) < 64
    ks = jnp.where(half, SCALE, -lam * SCALE)

    def main(j, c):
        dv, dk1, dk2 = keys_block(j, vn, qz1, qz2, kt, p1, p2, aa, dot, do, delta, dqt)
        rows = pl.ds(pl.multiple_of(j * B, B), B)
        gv[rows, :] = dv.astype(BF)
        gk[rows, :] = ((dk1 + dk2) * ks).astype(BF)
        return c
    lax.fori_loop(0, NB, main, 0)

    def fin(i, c):
        rows = pl.ds(pl.multiple_of(i * B, B), B)
        gq[rows, :] = (dqt[i].T * ks).astype(BF)
        return c
    lax.fori_loop(0, NB, fin, 0)


def body(tokens, cotangent, value_weight, query_heads, key_heads, lambdas):
    L = query_heads.shape[1]
    sp, dp, r = lax.axis_size("sp"), lax.axis_size("dp"), value_weight.shape[0]
    q = query_heads.reshape(L, 128)
    k = key_heads.reshape(L, 128)
    wide = lax.all_gather(tokens, "sp", axis=1, tiled=True)[0]
    full = lax.all_gather(value_weight, ("sp", "dp"), axis=0, tiled=True)
    own = lax.all_to_all(value_weight, "sp", split_axis=1, concat_axis=0, tiled=True)
    wh = lax.all_gather(own.reshape(sp, r, 128), "dp", axis=1).reshape(sp * dp * r, 128)
    cot = lax.all_to_all(cotangent, "sp", split_axis=2, concat_axis=1, tiled=True)[0]
    smem = pl.BlockSpec(memory_space=pltpu.SMEM)
    vm = pl.BlockSpec(memory_space=pltpu.VMEM)
    tiles = (NB * (NB + 1) // 2, B, B)
    p1, p2, aa = pl.pallas_call(
        first_kernel, out_shape=(S(tiles, BF),) * 3, in_specs=[smem, vm, vm], out_specs=[vm] * 3,
        scratch_shapes=[V((NB, B, 128), BF), V((NB, B, 128), BF), V((NB, 128, B), BF), V((NB, B, B), F32), V((NB, B, B), F32)],
        compiler_params=pltpu.CompilerParams(vmem_limit_bytes=48 * 1024 * 1024),
        cost_estimate=pl.CostEstimate(flops=20_000_000_000, bytes_accessed=20_000_000, transcendentals=0),
        name="softmaxes")(lambdas, q, k)
    v = jnp.dot(wide, wh, preferred_element_type=F32).astype(BF)
    gq, gk, gv, gl = pl.pallas_call(
        second_kernel, out_shape=(S((L, 128), BF),) * 3 + (S((8, 128), F32),),
        in_specs=[smem] + [vm] * 7, out_specs=[vm] * 4,
        scratch_shapes=[V((NB, B, 128), BF), V((NB, B, 128), BF), V((NB, 128, B), BF), V((NB, 128, B), BF), V((NB, B, 128), BF),
                        V((NB, 128, B), BF), V((NB, B, 128), BF), V((NB, 8, B), F32), V((NB, 128, B), F32)],
        compiler_params=pltpu.CompilerParams(vmem_limit_bytes=48 * 1024 * 1024),
        cost_estimate=pl.CostEstimate(flops=50_000_000_000, bytes_accessed=20_000_000, transcendentals=0),
        name="gradients")(lambdas, q, k, v, cot, p1, p2, aa)
    lam_all = lax.all_gather(gl[0:1, 0], "dp", axis=0, tiled=True)
    grad_lambda = jnp.sum(lam_all).reshape(1)
    gvt = lax.all_to_all(gv[None], "sp", split_axis=1, concat_axis=2, tiled=True)[0]
    gt = lax.dot_general(gvt, full, (((1,), (1,)), ((), ())), preferred_element_type=F32).astype(BF)[None]
    part = lax.dot_general(wide, gv, (((0,), (0,)), ((), ())), preferred_element_type=F32).astype(BF)
    part = part.reshape(sp, dp, r, 128)
    got = lax.all_to_all(part, "dp", split_axis=1, concat_axis=1, tiled=True)
    summed = jnp.sum(got.astype(F32), axis=1).astype(BF)
    gw = lax.all_to_all(summed.reshape(sp * r, 128), "sp", split_axis=0, concat_axis=1, tiled=True).astype(F32)
    return gq.reshape(query_heads.shape), gk.reshape(key_heads.shape), gt, gw, grad_lambda


def solution(mesh):
    placed = (P("dp", "sp", None), P("dp", "sp", None), P(("sp", "dp"), None),
              P("dp", None, "sp", None), P("dp", None, "sp", None), P("sp"))
    outs = (P("dp", None, "sp", None), P("dp", None, "sp", None), P("dp", "sp", None), P(("sp", "dp"), None), P("sp"))
    return jax.shard_map(body, mesh=mesh, in_specs=placed, out_specs=outs, check_vma=False)
```

profile of v0, /device:TPU:1, one launch (start us, length us, event | category | flops | bytes accessed | tf_op | source)
XLA Modules:
  0.0 200.5 jit_solution(18306567274049906940)
XLA Ops:
  7.2 0.0 all-gather.5.cloned.1.call-start
  7.2 0.7 all-gather.5.cloned.1.call-update
  7.9 0.0 all-gather.7.cloned.1.call-start
  7.9 0.7 all-gather.7.cloned.1.call-update
  8.7 1.5 copy_bitcast_fusion.1
  10.1 8.6 %all-to-all-start = ((bf16[16,16,128]{2,0,1:T(8,128)(2,1)}), bf16[16,16,128]{2,0,1:T(8,128)(2,1)S(1)}, u32[]{:S(2)}, u32[]{:S(2)}) async-start(bf16[16,16,128]{2,0,1:T(8,128)(2,1)} %copy_bitcast_fusion.1), calls=%async_computation | async-start | bytes 131072 | tf_op jit(solution)/shard_map/all_to_all | solution.py:197
  19.4 2.4 %copy.31 = bf16[1,128,2048]{1,0,2:T(2,128)(2,1)S(1)} copy(bf16[1,128,2048]{2,1,0:T(8,128)(2,1)} %param.7) | data formatting | bytes 1048576 | tf_op args[1]
  21.7 0.5 broadcast.1
  22.2 11.5 %reduce.4 = bf16[2048,128]{1,0:T(8,128)(2,1)S(1)} reduce(bf16[2048,1,128]{2,1,0:T(2,128)(2,1)S(1)} %bitcast.66, bf16[]{:T(256)} %broadcast.1), dimensions={1}, to_apply=%bitcast.43.reduce_sub_computation | reduce | bytes 1048578
  33.8 0.9 reshape.61
  34.7 6.7 %all-to-all-start.1 = ((bf16[16,2,8192]{2,1,0:T(2,128)(2,1)}), bf16[16,2,8192]{2,1,0:T(2,128)(2,1)S(1)}, u32[]{:S(2)}, u32[]{:S(2)}) async-start(bf16[16,2,8192]{2,1,0:T(2,128)(2,1)} %reshape.61), calls=%async_computation.1 | async-start | bytes 1048576 | tf_op jit(solution)/shard_map/all_to_all | solution.py:199
  41.4 0.0 copy-start
  41.4 1.0 copy-done
  42.4 1.0 copy-done.2
  43.5 16.1 %softmaxes.1 = (bf16[36,256,256]{2,1,0:T(8,128)(2,1)S(1)}, bf16[36,256,256]{2,1,0:T(8,128)(2,1)}, bf16[36,256,256]{2,1,0:T(8,128)(2,1)}) custom-call(f32[1]{0:T(128)S(6)} %copy.49.lam_ref, bf16[2048,128]{1,0:T(8,128)(2,1)S(1)} %bitcast.58, bf16[2048,128]{1,0:T(8,128)(2,1)S(1)} %bitcast.60), custom_call_target="tpu_custom_call" | custom-call | flops 20000000000 | bytes 20000000 | tf_op jit(solution)/shard_map/softmaxes/pallas_call | solution.py:203
  59.5 2.2 %copy-done.4 = bf16[36,256,256]{2,1,0:T(8,128)(2,1)} copy-done((bf16[36,256,256]{2,1,0:T(8,128)(2,1)}, bf16[36,256,256]{2,1,0:T(8,128)(2,1)S(1)}, u32[]{:S(2)}) %copy-start.4) | copy-done | bytes 4718616
  61.8 15.0 %all-gather = bf16[16,128,128]{2,0,1:T(8,128)(2,1)S(1)} all-gather(bf16[16,16,128]{2,0,1:T(8,128)(2,1)S(1)} %copy.29), channel_id=2, replica_groups=mesh['sp'=16,'dp'=8] {'dp'}, dimensions={1}, use_global_device_ids=true | all-gather | bytes 589824 | tf_op jit(solution)/shard_map/all_gather | solution.py:198
  76.8 0.1 copy.30
  76.9 0.0 copy-start.1
  76.9 0.0 copy-start.3
  77.0 0.5 reshape.62
  77.5 0.1 copy.39
  77.6 0.3 copy.32
  77.9 8.7 %all-gather.5.cloned.1.call-done = bf16[1,2048,2048]{2,1,0:T(8,128)(2,1)} async-done(((bf16[1,128,2048]{2,1,0:T(8,128)(2,1)}), bf16[1,2048,2048]{2,1,0:T(8,128)(2,1)}) %all-gather.5.cloned.1.call-update) | async-done | bytes 8388624 | tf_op jit(solution)/shard_map/all_gather | solution.py:195
  86.6 5.9 %fusion.4.v_ref = bf16[2048,128]{1,0:T(8,128)(2,1)S(1)} fusion(bf16[2048,128]{1,0:T(8,128)(2,1)S(1)} %bitcast.72, bf16[1,2048,2048]{2,1,0:T(8,128)(2,1)} %all-gather.5.cloned.1.call-done), kind=kOutput, calls=%fused_computation.4 | convolution fusion | flops 1074003968 | bytes 9437184 | tf_op jit(solution)/shard_map/dot_general | solution.py:209
  92.5 29.7 %gradients.1 = (bf16[2048,128]{1,0:T(8,128)(2,1)}, bf16[2048,128]{1,0:T(8,128)(2,1)}, bf16[2048,128]{1,0:T(8,128)(2,1)S(1)}, f32[8,128]{1,0:T(8,128)S(1)}) custom-call(f32[1]{0:T(128)S(6)} %copy.49.lam_ref, bf16[2048,128]{1,0:T(8,128)(2,1)S(1)} %bitcast.59, bf16[2048,128]{1,0:T(8,128)(2,1)S(1)} %bitcast.61, bf16[2048,128]{1,0:T(8,128)(2,1)S(1)} %fusion.4.v_ref, ...), custom_call_target="tpu_custom_call" | custom-call | flops 49999998976 | bytes 20000000 | tf_op jit(solution)/shard_map/gradients/pallas_call | solution.py:210
  122.2 1.3 fusion.11
  123.5 0.0 copy-start.5
  123.5 0.3 copy.35
  123.8 0.9 copy.36
  124.7 4.8 %all-to-all-start.3 = ((bf16[16,8,16,128]{3,2,0,1:T(8,128)(2,1)}), bf16[16,8,16,128]{3,2,0,1:T(8,128)(2,1)S(1)}, u32[]{:S(2)}, u32[]{:S(2)}) async-start(bf16[16,8,16,128]{3,2,0,1:T(8,128)(2,1)} %copy.36), calls=%async_computation.3 | async-start | bytes 1048576 | tf_op jit(solution)/shard_map/all_to_all | solution.py:224
  129.5 8.1 %copy.47 = bf16[1,2048,128]{2,0,1:T(2,128)(2,1)S(1)} copy(bf16[1,2048,128]{2,1,0:T(8,128)(2,1)S(1)} %bitcast.56) | data formatting | bytes 1048576 | tf_op jit(solution)/shard_map/broadcast_in_dim | solution.py:220
  137.6 11.5 %reduce.5 = bf16[2048,128]{1,0:T(8,128)(2,1)S(1)} reduce(bf16[2048,1,128]{2,1,0:T(2,128)(2,1)S(1)} %bitcast.67, bf16[]{:T(256)} %broadcast.1), dimensions={1}, to_apply=%bitcast.55.reduce_sub_computation | reduce | bytes 1048578
  149.1 0.9 reshape.63
  150.1 3.8 %all-to-all-start.2 = ((bf16[16,2,8192]{2,1,0:T(2,128)(2,1)}), bf16[16,2,8192]{2,1,0:T(2,128)(2,1)S(1)}, u32[]{:S(2)}, u32[]{:S(2)}) async-start(bf16[16,2,8192]{2,1,0:T(2,128)(2,1)} %reshape.63), calls=%async_computation.2 | async-start | bytes 1048576 | tf_op jit(solution)/shard_map/all_to_all | solution.py:220
  153.9 0.7 reduce_sum.21
  154.6 10.3 %all-to-all-done.2 = bf16[16,2,8192]{2,1,0:T(2,128)(2,1)S(1)} async-done(((bf16[16,2,8192]{2,1,0:T(2,128)(2,1)}), bf16[16,2,8192]{2,1,0:T(2,128)(2,1)S(1)}, u32[]{:S(2)}, u32[]{:S(2)}) %all-to-all-start.2) | async-done | bytes 524320 | tf_op jit(solution)/shard_map/all_to_all | solution.py:220
  164.9 3.5 %all-to-all-start.4 = ((bf16[16,16,128]{2,1,0:T(8,128)(2,1)}), bf16[16,16,128]{2,1,0:T(8,128)(2,1)S(1)}, u32[]{:S(2)}, u32[]{:S(2)}) async-start(bf16[16,16,128]{2,1,0:T(8,128)(2,1)} %reduce_sum.21), calls=%async_computation.4 | async-start | bytes 131072 | tf_op jit(solution)/shard_map/all_to_all | solution.py:226
  168.4 0.6 dynamic-slice
  169.0 0.5 slice.3
  169.5 1.3 bitcast_dynamic-update-slice_fusion
  170.9 13.5 %all-reduce = f32[8]{0:T(128)S(1)} all-reduce(f32[8]{0:T(128)S(1)} %bitcast_dynamic-update-slice_fusion), channel_id=3, replica_groups=mesh['sp'=16,'dp'=8] {'dp'}, use_global_device_ids=true, to_apply=%add | all-reduce | flops 8 | bytes 64
  184.4 0.6 reduce.2
  185.0 0.5 reshape.64
  185.5 0.1 copy.40
  185.6 0.3 copy.34
  185.9 0.7 copy_bitcast_fusion
  186.5 7.1 %fusion.10 = bf16[1,128,2048]{2,1,0:T(8,128)(2,1)} fusion(bf16[128,2048]{0,1:T(8,128)(2,1)S(1)} %bitcast.68, bf16[2048,2048]{1,0:T(8,128)(2,1)} %all-gather.7.cloned.1.call-done), kind=kOutput, calls=%fused_computation.7 | convolution fusion | flops 1074003968 | bytes 9437184 | tf_op jit(solution)/shard_map/dot_general | solution.py:221
  (17 shorter events, 0.1 us)
Async XLA Ops:
  7.2 79.4 %all-gather.5.cloned.1.call-start = ((), (), s32[]{:S(2)}) async-start(), calls=%async_computation.5 | async-start | bytes 8912896 | tf_op jit(solution)/shard_map/all_gather | solution.py:195
  7.9 178.6 %all-gather.7.cloned.1.call-start = ((), (), s32[]{:S(2)}) async-start(), calls=%async_computation.6 | async-start | bytes 8454144 | tf_op jit(solution)/shard_map/all_gather | solution.py:196
  10.1 24.6 %all-to-all-start = ((bf16[16,16,128]{2,0,1:T(8,128)(2,1)}), bf16[16,16,128]{2,0,1:T(8,128)(2,1)S(1)}, u32[]{:S(2)}, u32[]{:S(2)}) async-start(bf16[16,16,128]{2,0,1:T(8,128)(2,1)} %copy_bitcast_fusion.1), calls=%async_computation | async-start | bytes 131072 | tf_op jit(solution)/shard_map/all_to_all | solution.py:197
  34.7 42.3 %all-to-all-start.1 = ((bf16[16,2,8192]{2,1,0:T(2,128)(2,1)}), bf16[16,2,8192]{2,1,0:T(2,128)(2,1)S(1)}, u32[]{:S(2)}, u32[]{:S(2)}) async-start(bf16[16,2,8192]{2,1,0:T(2,128)(2,1)} %reshape.61), calls=%async_computation.1 | async-start | bytes 1048576 | tf_op jit(solution)/shard_map/all_to_all | solution.py:199
  41.4 1.0 copy-start
  42.4 1.0 copy-start.2
  59.5 2.2 %copy-start.4 = (bf16[36,256,256]{2,1,0:T(8,128)(2,1)}, bf16[36,256,256]{2,1,0:T(8,128)(2,1)S(1)}, u32[]{:S(2)}) copy-start(bf16[36,256,256]{2,1,0:T(8,128)(2,1)S(1)} %get-tuple-element.12.p1) | copy-start | bytes 14155780
  76.9 15.6 %copy-start.1 = (bf16[1,2048,1,128]{3,1,2,0:T(8,128)(2,1)S(1)}, bf16[1,2048,1,128]{3,1,2,0:T(8,128)(2,1)}, u32[]{:S(2)}) copy-start(bf16[1,2048,1,128]{3,1,2,0:T(8,128)(2,1)} %param.9) | copy-start | bytes 1572868
  76.9 15.6 %copy-start.3 = (bf16[1,2048,1,128]{3,1,2,0:T(8,128)(2,1)S(1)}, bf16[1,2048,1,128]{3,1,2,0:T(8,128)(2,1)}, u32[]{:S(2)}) copy-start(bf16[1,2048,1,128]{3,1,2,0:T(8,128)(2,1)} %param.10) | copy-start | bytes 1572868
  86.6 35.6 %slice-start = ((s8[8388608]{0:T(1024)(128)(4,1)}), s8[4194304]{0:T(1024)(128)(4,1)S(1)}, s32[]{:S(2)}) async-start(s8[8388608]{0:T(1024)(128)(4,1)} %bitcast.62), calls=%async_computation.7 | async-start | bytes 8388608
  92.5 29.7 %slice-start.1 = ((s8[8388608]{0:T(1024)(128)(4,1)}), s8[4194304]{0:T(1024)(128)(4,1)S(1)}, s32[]{:S(2)}) async-start(s8[8388608]{0:T(1024)(128)(4,1)} %bitcast.62), calls=%async_computation.8 | async-start | bytes 8388608
  123.5 44.9 %copy-start.5 = (u32[128]{0:T(128)S(1)}, u32[128]{0:T(128)}, u32[]{:S(2)}) copy-start(u32[128]{0:T(128)} %constant.12) | copy-start | bytes 1540
  124.7 25.4 %all-to-all-start.3 = ((bf16[16,8,16,128]{3,2,0,1:T(8,128)(2,1)}), bf16[16,8,16,128]{3,2,0,1:T(8,128)(2,1)S(1)}, u32[]{:S(2)}, u32[]{:S(2)}) async-start(bf16[16,8,16,128]{3,2,0,1:T(8,128)(2,1)} %copy.36), calls=%async_computation.3 | async-start | bytes 1048576 | tf_op jit(solution)/shard_map/all_to_all | solution.py:224
  150.1 14.9 %all-to-all-start.2 = ((bf16[16,2,8192]{2,1,0:T(2,128)(2,1)}), bf16[16,2,8192]{2,1,0:T(2,128)(2,1)S(1)}, u32[]{:S(2)}, u32[]{:S(2)}) async-start(bf16[16,2,8192]{2,1,0:T(2,128)(2,1)} %reshape.63), calls=%async_computation.2 | async-start | bytes 1048576 | tf_op jit(solution)/shard_map/all_to_all | solution.py:220
  164.9 20.9 %all-to-all-start.4 = ((bf16[16,16,128]{2,1,0:T(8,128)(2,1)}), bf16[16,16,128]{2,1,0:T(8,128)(2,1)S(1)}, u32[]{:S(2)}, u32[]{:S(2)}) async-start(bf16[16,16,128]{2,1,0:T(8,128)(2,1)} %reduce_sum.21), calls=%async_computation.4 | async-start | bytes 131072 | tf_op jit(solution)/shard_map/all_to_all | solution.py:226
Sparse Core Ops, SparseCore 0:
  10.1 76.4 all-gather.4
  89.6 69.5 all-gather.6
where the time goes:
time: 202 us; the launch traced here: 200 us
  Pallas kernels  45.8 us (23%)
  blocking collectives  28.5 us (14%)
  starting transfers between devices  27.4 us (14%)
  other arithmetic  25 us (12%)
  local copies, waits for them, and re-layouts  24.1 us (12%)
  waiting for transfers between devices  20.4 us (10%)
  between operations  14.9 us (7%)
  matrix products  14.3 us (7%)
    pallas_call x1, Pallas kernels, body(): pl.pallas_call(second_kernel, out_shape=(S((L, 128), BF),) * 3 + (S((8, 1...  29.7 us
    unnamed x3, other arithmetic  23.1 us
    pallas_call x1, Pallas kernels, body(): pl.pallas_call(first_kernel, out_shape=(S(tiles, BF),) * 3, in_specs=[sme...  16.1 us
    all_gather x1, blocking collectives, body(): lax.all_gather(own.reshape(sp, r, 128), 'dp', axis=1)  15 us
    unnamed x1, blocking collectives  13.5 us
    unnamed x27, local copies, waits for them, and re-layouts  12.1 us
    all_to_all x1, waiting for transfers between devices, body(): lax.all_to_all(gv[None], 'sp', split_axis=1, concat_axis=2, tiled=True)[0]  10.3 us
    all_gather x1, waiting for transfers between devices, body(): wide = lax.all_gather(tokens, 'sp', axis=1, tiled=True)[0]  8.7 us
  transfers between devices with their start and end apart: 7, of which 2 were waited for; matrix products, arithmetic and copies ran while one was open for 26% of the time, Pallas kernels for 23%

commit v1 on v0

v1 whole, which is shorter than its diff:
```python
import functools, math
import jax, jax.numpy as jnp
from jax import lax
from jax.experimental import pallas as pl
from jax.experimental.pallas import tpu as pltpu
from jax.sharding import PartitionSpec as P

EPS = 1e-6
B = 256
NB = 8
SCALE = 0.125
LOG2E = 1.4426950408889634
F32 = jnp.float32
BF = jnp.bfloat16

def nt(a, b):
    return lax.dot_general(a, b, (((1,), (1,)), ((), ())), preferred_element_type=F32)

def nn(a, b):
    return lax.dot_general(a, b, (((1,), (0,)), ((), ())), preferred_element_type=F32)

def tri(i, j):
    return (i * (i + 1)) // 2 + j

def paired(lo, n, body):
    def two(p, c):
        body(lo + 2 * p, 2)
        return c
    lax.fori_loop(0, n // 2, two, 0)
    def one(p, c):
        body(lo + n - 1, 1)
        return c
    lax.fori_loop(0, n % 2, one, 0)

def prepare(i, q_ref, k_ref, qz1, qz2, kt):
    rows = pl.ds(pl.multiple_of(i * B, B), B)
    q = q_ref[rows, :]
    first = lax.broadcasted_iota(jnp.int32, (B, 128), 1) < 64
    zero = jnp.zeros_like(q)
    qz1[i] = jnp.where(first, q, zero)
    qz2[i] = jnp.where(first, zero, q)
    kt[i] = k_ref[rows, :].T

def softmaxes(i, lam, k_ref, qz1, qz2, s1, s2, p1, p2, aa):
    q1, q2 = qz1[i], qz2[i]

    def score(j, m):
        k = k_ref[pl.ds(pl.multiple_of(j * B, B), B), :]
        a, b = nt(k, q1), nt(k, q2)
        return a, b

    def keep(j, a, b, m):
        s1[j] = a
        s2[j] = b
        return (jnp.maximum(m[0], jnp.max(a.reshape(B // 8, 8, B), axis=0)),
                jnp.maximum(m[1], jnp.max(b.reshape(B // 8, 8, B), axis=0)))

    a, b = score(i, None)
    seen = lax.broadcasted_iota(jnp.int32, (B, B), 0) <= lax.broadcasted_iota(jnp.int32, (B, B), 1)
    a = jnp.where(seen, a, -1e30)
    b = jnp.where(seen, b, -1e30)
    low = jnp.full((8, B), -1e30, F32)
    m = keep(i, a, b, (low, low))

    def off(j, m):
        a, b = score(j, m)
        return keep(j, a, b, m)
    def two(p, m):
        a, b = score(2 * p, m)
        c, d = score(2 * p + 1, m)
        m = keep(2 * p, a, b, m)
        return keep(2 * p + 1, c, d, m)
    m = lax.fori_loop(0, i // 2, two, m)
    m = lax.fori_loop(i - i % 2, i, off, m)
    m1 = jnp.max(m[0], axis=0, keepdims=True)
    m2 = jnp.max(m[1], axis=0, keepdims=True)
    c = SCALE * LOG2E

    def power(j, l):
        e1 = jnp.exp2((s1[j] - m1) * c)
        e2 = jnp.exp2((s2[j] - m2) * c)
        s1[j] = e1
        s2[j] = e2
        return (l[0] + jnp.sum(e1.reshape(B // 8, 8, B), axis=0),
                l[1] + jnp.sum(e2.reshape(B // 8, 8, B), axis=0))
    l = lax.fori_loop(0, i + 1, power, (jnp.zeros((8, B), F32), jnp.zeros((8, B), F32)))
    r1 = 1.0 / jnp.sum(l[0], axis=0, keepdims=True)
    r2 = 1.0 / jnp.sum(l[1], axis=0, keepdims=True)

    def norm(j, _):
        x1 = s1[j] * r1
        x2 = s2[j] * r2
        t = tri(i, j)
        p1[t] = x1.astype(BF)
        p2[t] = x2.astype(BF)
        aa[t] = (x1 - lam * x2).astype(BF)
        return _
    lax.fori_loop(0, i + 1, norm, 0)

def keys_block(j, vn, qz1, qz2, kt, p1, p2, aa, dot, do, delta, dqt):
    v = vn[j]
    k1t, k2t = kt[j, 0:64, :], kt[j, 64:128, :]

    def parts(i):
        t = tri(i, j)
        da = nn(v, dot[i])
        x1 = (p1[t].astype(F32) * (da - delta[i, 0:1, :])).astype(BF)
        x2 = (p2[t].astype(F32) * (da - delta[i, 1:2, :])).astype(BF)
        dv = nn(aa[t], do[i])
        dk1 = nn(x1, qz1[i])
        dk2 = nn(x2, qz2[i])
        dqt[i, 0:64, :] += nn(k1t, x1)
        dqt[i, 64:128, :] += nn(k2t, x2)
        return dv, dk1 , dk2

    def two(p, c):
        a = parts(j + 2 * p)
        b = parts(j + 2 * p + 1)
        return tuple(x + (y + z) for x, y, z in zip(c, a, b))
    def one(p, c):
        a = parts(p)
        return tuple(x + y for x, y in zip(c, a))
    n = NB - j
    zero = jnp.zeros((B, 128), F32)
    c = lax.fori_loop(0, n // 2, two, (zero, zero, zero))
    c = lax.fori_loop(NB - n % 2, NB, one, c)
    return c[0], c[1], c[2]


MESH = pl.DeviceIdType.MESH
V = pltpu.VMEM
S = jax.ShapeDtypeStruct


class Plane:
    def __init__(self, at, ss, rs, sp, dp):
        self.at, self.ss, self.rs, self.dp = at, ss, rs, dp
        self.pos = (lax.rem(sp, 4), lax.div(sp, 4))

    def block(self, k, o, p):
        a = lax.rem(self.pos[k] + (o + 4), 4)
        b = lax.rem(self.pos[1 - k] + (p + 4), 4)
        return b * 4 + a if k == 0 else a * 4 + b

    def copy(self, k, slot, o, p, part, axis, delta):
        s = self.block(k, o, p)
        cols = pl.ds(k * 1024 + (512 if part == 2 else 0), 1024 if part == 0 else 512)
        to = self.block(0, delta, 0) if axis == 0 else self.block(0, 0, delta)
        return pltpu.make_async_remote_copy(
            src_ref=self.at(s, cols), dst_ref=self.at(s, cols), send_sem=self.ss.at[k, slot], recv_sem=self.rs.at[k, slot],
            device_id={"sp": to, "dp": self.dp}, device_id_type=MESH)

    def first(self):
        for k in (0, 1):
            self.copy(k, 0, 0, 0, 0, k, 1).start()
            self.copy(k, 1, 0, 0, 0, k, -1).start()

    def second(self, k, n):
        o = (0, -1, 1, 2)[n]
        self.copy(k, 4 + 4 * n, o, 0, 0, 1 - k, 1).start()
        self.copy(k, 5 + 4 * n, o, 0, 0, 1 - k, -1).start()

    def near(self):
        for k in (0, 1):
            self.copy(k, 0, -1, 0, 0, k, 1).wait_recv()
            self.copy(k, 2, -1, 0, 1, k, 1).start()
            self.copy(k, 1, 1, 0, 0, k, -1).wait_recv()
            self.copy(k, 3, 1, 0, 2, k, -1).start()
        for k in (0, 1):
            self.second(k, 1)
        for k in (0, 1):
            self.second(k, 2)

    def far(self):
        for k in (0, 1):
            self.copy(k, 2, 2, 0, 1, k, 1).wait_recv()
            self.copy(k, 3, 2, 0, 2, k, 1).wait_recv()
            self.second(k, 3)

    def across(self, n):
        o = (0, -1, 1, 2)[n]
        for k in (0, 1):
            self.copy(k, 4 + 4 * n, o, -1, 0, 1 - k, 1).wait_recv()
            self.copy(k, 6 + 4 * n, o, -1, 1, 1 - k, 1).start()
            self.copy(k, 5 + 4 * n, o, 1, 0, 1 - k, -1).wait_recv()
            self.copy(k, 7 + 4 * n, o, 1, 2, 1 - k, -1).start()

    def last(self, n):
        o = (0, -1, 1, 2)[n]
        for k in (0, 1):
            self.copy(k, 6 + 4 * n, o, 2, 1, 1 - k, 1).wait_recv()
            self.copy(k, 7 + 4 * n, o, 2, 2, 1 - k, 1).wait_recv()

    def drain(self):
        for k in (0, 1):
            for slot in range(20):
                self.copy(k, slot, 0, 0, 0 if slot % 4 < 2 else 1, 0, 1).wait_send()


class Row:
    def __init__(self, w, ss, rs, sp, dp):
        self.w, self.ss, self.rs, self.sp, self.dp = w, ss, rs, sp, dp
        self.x, self.c = lax.div(dp, 2), lax.rem(dp, 2)

    def own(self, o):
        return 2 * lax.rem(self.x + (o + 4), 4) + self.c

    def copy(self, slot, o, to, half=None):
        part = pl.ds(0, 16) if half is None else pl.ds(8 * half, 8)
        return pltpu.make_async_remote_copy(
            src_ref=self.w.at[part, self.own(o)], dst_ref=self.w.at[part, self.own(o)],
            send_sem=self.ss.at[slot], recv_sem=self.rs.at[slot],
            device_id={"sp": self.sp, "dp": to}, device_id_type=MESH)

    def other(self, slot, o):
        return self.copy(slot, o, self.dp + 1 - 2 * self.c)

    def start(self):
        self.copy(0, 0, self.own(1)).start()
        self.copy(1, 0, self.own(-1)).start()
        self.other(4, 0).start()

    def near(self):
        self.copy(0, -1, self.own(1)).wait_recv()
        self.copy(2, -1, self.own(1), 0).start()
        self.other(5, -1).start()
        self.copy(1, 1, self.own(-1)).wait_recv()
        self.copy(3, 1, self.own(-1), 1).start()
        self.other(6, 1).start()

    def far(self):
        self.copy(2, 2, self.own(1), 0).wait_recv()
        self.copy(3, 2, self.own(1), 1).wait_recv()
        self.other(7, 2).start()

    def finish(self):
        for slot in (4, 5, 6, 7):
            self.other(slot, 0).wait_recv()
        for slot in (0, 1, 4, 5, 6, 7):
            self.copy(slot, 0, self.own(1)).wait_send()
        for slot in (2, 3):
            self.copy(slot, 0, self.own(1), 0).wait_send()


def kernel(lam_ref, tok_h, cot_h, w_h, q_h, k_h, gq_h, gk_h, gt_h, gw_h, gl_h,
           x, w, wh, cota, q_ref, k_ref, qz1, qz2, kt, vt, vn, s1, s2, p1, p2, aa, dot, do, delta, dqt, ot, o2t,
           dvb, dvrow, gwt, gwp, gwin, gws, gwf, gqb, gkb, gtb, gwo, glb, glin,
           load, save, xs, xr, ws, wr, rs_, rr, h1s, h1r, h2s, h2r, cs, cr, ds_, dr, es, er, ls, lr, fs, fr):
    sp, dp = lax.axis_index("sp"), lax.axis_index("dp")
    lam = lam_ref[0]

    def sp_peers(body):
        lax.fori_loop(1, 16, lambda d, c: (body(lax.rem(sp + d, 16)), c)[1], 0)

    def dp_peers(body):
        lax.fori_loop(1, 8, lambda d, c: (body(lax.rem(dp + d, 8)), c)[1], 0)

    def remote(src, dst, ss, rs, s, d):
        return pltpu.make_async_remote_copy(src_ref=src, dst_ref=dst, send_sem=ss, recv_sem=rs,
                                            device_id={"sp": s, "dp": d}, device_id_type=MESH)

    def lanes(h):
        return pl.ds(pl.multiple_of(h * 128, 128), 128)

    def rows(i, n=B):
        return pl.ds(pl.multiple_of(i * n, n), n)

    barrier = pltpu.get_barrier_semaphore()
    sp_peers(lambda s: pl.semaphore_signal(barrier, inc=1, device_id={"sp": s, "dp": dp}, device_id_type=MESH))
    dp_peers(lambda d: pl.semaphore_signal(barrier, inc=1, device_id={"sp": sp, "dp": d}, device_id_type=MESH))
    loads = [pltpu.make_async_copy(a, b, load.at[n]) for n, (a, b) in enumerate((
        (w_h, w.at[sp, dp]), (tok_h, x.at[sp]), (q_h, q_ref), (k_h, k_ref), (cot_h.at[:, lanes(sp)], cota.at[rows(sp, 128)])))]
    for a in loads:
        a.start()
    wplane = Plane(lambda s, cols: w.at[s, dp, :, cols], ws, wr, sp, dp)
    xplane = Plane(lambda s, cols: x.at[s, :, cols], xs, xr, sp, dp)
    wrow = Row(w, rs_, rr, sp, dp)
    loads[0].wait()
    wh[sp, dp] = w[sp, dp, :, lanes(sp)]
    loads[1].wait()
    pl.semaphore_wait(barrier, 22)

    wplane.first()

    def part_of(s, src, dst):
        return remote(w.at[sp, dp, :, lanes(src)], wh.at[dst, dp], h1s.at[src], h1r.at[dst], s, dp)
    sp_peers(lambda s: part_of(s, s, sp).start())
    xplane.first()
    for k in (0, 1):
        wplane.second(k, 0)
    for n in (2, 3):
        loads[n].wait()

    def prep(i, c):
        prepare(i, q_ref, k_ref, qz1, qz2, kt)
        zero = jnp.zeros((128, B), F32)
        dqt[i] = zero
        ot[i] = zero
        o2t[i] = zero
        return c
    lax.fori_loop(0, NB, prep, 0)

    def soft(lo, hi):
        lax.fori_loop(lo, hi, lambda i, c: (softmaxes(i, lam, k_ref, qz1, qz2, s1, s2, p1, p2, aa), c)[1], 0)

    wplane.near()
    for k in (0, 1):
        xplane.second(k, 0)

    sp_peers(lambda s: part_of(s, sp, s).wait_recv())

    def column(d, src):
        return remote(wh.at[:, src], wh.at[:, src], h2s.at[d], h2r.at[src], sp, d)
    dp_peers(lambda d: column(d, dp).start())
    soft(0, 3)
    for n in (0,):
        wplane.across(n)
    wplane.far()
    xplane.near()
    soft(3, 5)
    for n in (1, 2, 3):
        wplane.across(n)
    xplane.across(0)
    xplane.far()
    soft(5, 6)
    for n in range(4):
        wplane.last(n)
    wrow.start()
    soft(6, 8)
    dp_peers(lambda d: column(dp, d).wait_recv())

    def values(j):
        v = nn(x[pl.ds(2 * j, 2)].reshape(B, 2048), wh[...].reshape(2048, 128)).astype(BF)
        vn[j] = v
        v = v.T
        vt[j] = v

        def add(i, count):
            for m in range(count):
                t = tri(i + m, j)
                ot[i + m] += nn(v, aa[t])
                o2t[i + m] += nn(v, p2[t])
        paired(j, NB - j, add)

    y, z = lax.rem(sp, 4), lax.div(sp, 4)
    side = lax.div(y, 2)

    def pair(dz, which):
        return 2 * lax.rem(z + dz, 4) + (side if which == 0 else 1 - side)
    many = lambda js: lax.fori_loop(0, len(js), lambda n, c: (values(sum(jnp.where(n == m, j, 0) for m, j in enumerate(js))), c)[1], 0)

    many([pair(0, 0)])
    xplane.across(1)
    xplane.across(2)
    many([pair(1, 0), pair(3, 0)])
    xplane.last(0)
    many([pair(0, 1)])
    xplane.across(3)

    def cot_part(s, src, dst):
        return remote(cot_h.at[:, lanes(src)], cota.at[rows(dst, 128)], cs.at[src], cr.at[dst], s, dp)
    sp_peers(lambda s: cot_part(s, s, sp).start())
    xplane.last(1)
    xplane.last(2)
    many([pair(1, 1), pair(3, 1), pair(2, 0)])
    xplane.last(3)
    many([pair(2, 1)])
    wrow.near()
    loads[4].wait()
    sp_peers(lambda s: cot_part(s, sp, s).wait_recv())

    def mix(i, total):
        o, o2 = ot[i], o2t[i]
        g = cota[rows(i), :].astype(F32).T
        r = lax.rsqrt(jnp.mean(o * o, axis=0, keepdims=True) + EPS)
        yy = r * o
        d = (r * (g - yy * jnp.mean(g * yy, axis=0, keepdims=True))).astype(BF)
        dw = d.astype(F32)
        d2 = jnp.sum(dw * o2, axis=0, keepdims=True)
        d1 = jnp.sum(dw * o, axis=0, keepdims=True) + lam * d2
        dot[i] = d
        do[i] = dw.T.astype(BF)
        delta[i, 0:1, :] = d1
        delta[i, 1:2, :] = d2
        return total + d2
    total = lax.fori_loop(0, NB, mix, jnp.zeros((1, B), F32))
    glb[...] = jnp.broadcast_to(-jnp.sum(total, axis=1, keepdims=True), (8, 128))
    gwt[...] = jnp.zeros_like(gwt)

    half = lax.broadcasted_iota(jnp.int32, (1, 128), 1) < 64
    ks = jnp.where(half, SCALE, -lam * SCALE)

    def dv_part(s, t, src):
        return remote(dvb.at[t], dvrow.at[:, lanes(src)], ds_.at[t], dr.at[src], s, dp)

    def main(j, c):
        dv, dk1, dk2 = keys_block(j, vn, qz1, qz2, kt, p1, p2, aa, dot, do, delta, dqt)
        gkb[rows(j), :] = ((dk1 + dk2) * ks).astype(BF)
        dvt = dv.T.astype(BF)
        dvl = dv.astype(BF)
        dvb[2 * j] = dvl[:128]
        dvb[2 * j + 1] = dvl[128:]
        for n in range(4):
            cols = pl.ds(n * 512, 512)
            gwt[:, cols] += nn(dvt, x[pl.ds(2 * j, 2), :, cols].reshape(B, 512))
        for e in range(2):
            t = 2 * j + e

            @pl.when(t != sp)
            def _():
                dv_part(t, t, sp).start()
        return c
    lax.fori_loop(0, NB, main, 0)
    dvrow[:, lanes(sp)] = dvb[sp]

    def out_rows(n, c):
        part = gwt[:, rows(n, 128)].T.astype(BF)
        gwp[n] = part.reshape(8, 16, 128)
        return c
    lax.fori_loop(0, 16, out_rows, 0)

    def gw_part(d, to, src):
        return remote(gwp.at[:, to], gwin.at[src], es.at[to], er.at[src], sp, d)

    def gl_part(d, to, src):
        return remote(glb, glin.at[src], ls.at[to], lr.at[src], sp, d)
    dp_peers(lambda d: gw_part(d, d, dp).start())
    dp_peers(lambda d: gl_part(d, d, dp).start())
    gwin[dp] = gwp[:, dp]
    glin[dp] = glb[...]

    save_k = pltpu.make_async_copy(gkb, gk_h, save.at[0])
    save_k.start()
    wrow.far()

    def fin(i, c):
        gqb[rows(i), :] = (dqt[i].T * ks).astype(BF)
        return c
    lax.fori_loop(0, NB, fin, 0)
    save_q = pltpu.make_async_copy(gqb, gq_h, save.at[1])
    save_q.start()
    sp_peers(lambda s: dv_part(s, s, s).wait_recv())
    wrow.finish()

    def tokens_grad(n, c):
        g = nt(dvrow[...], w[pl.ds(2 * n, 2)].reshape(B, 2048))
        gtb[:, rows(n)] = g.astype(BF)
        return c
    lax.fori_loop(0, NB, tokens_grad, 0)
    save_t = pltpu.make_async_copy(gtb, gt_h, save.at[2])
    save_t.start()

    dp_peers(lambda d: gw_part(d, d, d).wait_recv())
    acc = gwin[0].astype(F32)
    for d in range(1, 8):
        acc = acc + gwin[d].astype(F32)
    gws[...] = acc.astype(BF)

    def fin_part(s, to, src):
        return remote(gws.at[to], gwf.at[src], fs.at[to], fr.at[src], s, dp)
    sp_peers(lambda s: fin_part(s, s, sp).start())
    gwf[sp] = gws[sp]
    dp_peers(lambda d: gl_part(d, d, d).wait_recv())
    tot = glin[0]
    for d in range(1, 8):
        tot = tot + glin[d]
    glb2 = delta
    glb2[0] = jnp.concatenate([tot, tot], axis=1)
    save_l = pltpu.make_async_copy(glb2.at[0, :, pl.ds(0, 128)], gl_h, save.at[3])
    save_l.start()
    xplane.drain()
    wplane.drain()
    sp_peers(lambda s: part_of(s, s, sp).wait_send())
    dp_peers(lambda d: column(d, dp).wait_send())
    sp_peers(lambda s: cot_part(s, s, sp).wait_send())
    sp_peers(lambda s: dv_part(s, s, sp).wait_send())
    dp_peers(lambda d: gw_part(d, d, dp).wait_send())
    dp_peers(lambda d: gl_part(d, d, dp).wait_send())
    sp_peers(lambda s: fin_part(s, s, s).wait_recv())
    for h in range(16):
        gwo[:, h * 128:(h + 1) * 128] = gwf[h].astype(F32)
    save_w = pltpu.make_async_copy(gwo, gw_h, save.at[4])
    save_w.start()
    sp_peers(lambda s: fin_part(s, s, sp).wait_send())
    for a in (save_k, save_q, save_t, save_l, save_w):
        a.wait()


def body(tokens, cotangent, value_weight, query_heads, key_heads, lambdas):
    L = query_heads.shape[1]
    smem = pl.BlockSpec(memory_space=pltpu.SMEM)
    anywhere = pl.BlockSpec(memory_space=pl.ANY)
    tiles = (NB * (NB + 1) // 2, B, B)
    dma = lambda *n: pltpu.SemaphoreType.DMA(n)
    gq, gk, gt, gw, gl = pl.pallas_call(
        kernel,
        out_shape=(S((L, 128), BF), S((L, 128), BF), S((128, 2048), BF), S((16, 2048), F32), S((8, 128), F32)),
        in_specs=[smem] + [anywhere] * 5, out_specs=[anywhere] * 5,
        scratch_shapes=[
            V((16, 128, 2048), BF), V((16, 8, 16, 2048), BF), V((16, 8, 16, 128), BF), V((L, 128), BF), V((L, 128), BF), V((L, 128), BF),
            V((NB, B, 128), BF), V((NB, B, 128), BF), V((NB, 128, B), BF), V((NB, 128, B), BF), V((NB, B, 128), BF),
            V((NB, B, B), F32), V((NB, B, B), F32), V(tiles, BF), V(tiles, BF), V(tiles, BF),
            V((NB, 128, B), BF), V((NB, B, 128), BF), V((NB, 8, B), F32), V((NB, 128, B), F32), V((NB, 128, B), F32), V((NB, 128, B), F32),
            V((16, 128, 128), BF), V((128, 2048), BF), V((128, 2048), F32), V((16, 8, 16, 128), BF), V((8, 16, 16, 128), BF),
            V((16, 16, 128), BF), V((16, 16, 128), BF), V((L, 128), BF), V((L, 128), BF), V((128, 2048), BF), V((16, 2048), F32),
            V((8, 128), F32), V((8, 8, 128), F32),
            dma(5), dma(5), dma(2, 20), dma(2, 20), dma(2, 20), dma(2, 20), dma(8), dma(8), dma(16), dma(16), dma(8), dma(8),
            dma(16), dma(16), dma(16), dma(16), dma(8), dma(8), dma(8), dma(8), dma(16), dma(16)],
        compiler_params=pltpu.CompilerParams(vmem_limit_bytes=60 * 1024 * 1024, collective_id=0, has_side_effects=True),
        name="whole")(lambdas, tokens[0], cotangent[0], value_weight, query_heads.reshape(L, 128), key_heads.reshape(L, 128))
    return gq.reshape(query_heads.shape), gk.reshape(key_heads.shape), gt[None], gw, gl[0, 0:1]


def solution(mesh):
    placed = (P("dp", "sp", None), P("dp", "sp", None), P(("sp", "dp"), None),
              P("dp", None, "sp", None), P("dp", None, "sp", None), P("sp"))
    outs = (P("dp", None, "sp", None), P("dp", None, "sp", None), P("dp", "sp", None), P(("sp", "dp"), None), P("sp"))
    return jax.shard_map(body, mesh=mesh, in_specs=placed, out_specs=outs, check_vma=False)
```

time: 202 us -> 109 us (0.54)
  Pallas kernels: 45.8 us -> 99.9 us
  blocking collectives: 28.5 us -> 0 us
  starting transfers between devices: 27.4 us -> 0 us
  other arithmetic: 25 us -> 0 us
  waiting for transfers between devices: 20.4 us -> 0 us
  local copies, waits for them, and re-layouts: 24.1 us -> 6.03 us
  matrix products: 14.3 us -> 0 us
  between operations: 14.9 us -> 1.29 us
    pallas_call x2 -> x1, Pallas kernels: 45.8 us -> 99.9 us  [body(): pl.pallas_call(kernel, out_shape=(S((L, 128), BF), S((L, 128), BF), S((12...]
    all_to_all x5 -> x0, starting transfers between devices: 27.4 us -> none  [the longest x1 8.59 us: body(): lax.all_to_all(value_weight, 'sp', split_axis=1, concat_axis=0, tiled=True)]
    unnamed x3 -> x0, other arithmetic: 23.1 us -> none
    all_gather x1 -> x0, blocking collectives: 15 us -> none  [body(): lax.all_gather(own.reshape(sp, r, 128), 'dp', axis=1)]
    dot_general x3 -> x0, matrix products: 14.3 us -> none  [the longest x1 7.09 us: body(): lax.dot_general(gvt, full, (((1,), (1,)), ((), ())), preferred_element_ty...]
    unnamed x1 -> x0, blocking collectives: 13.5 us -> none
    all_to_all x5 -> x0, waiting for transfers between devices: 10.3 us -> none  [the longest x1 10.3 us: body(): lax.all_to_all(gv[None], 'sp', split_axis=1, concat_axis=2, tiled=True)[0]]
    all_gather x2 -> x0, waiting for transfers between devices: 8.7 us -> none  [the longest x1 8.7 us: body(): wide = lax.all_gather(tokens, 'sp', axis=1, tiled=True)[0]]
  transfers between devices with their start and end apart: 7 -> 0, of which waited for: 2 -> 0; matrix products, arithmetic and copies ran while one was open for 26% -> 0% of each run, Pallas kernels for 23% -> 0%
where the time goes in v1:
time: 109 us; the launch traced here: 107 us
  Pallas kernels  99.9 us (92%)
  local copies, waits for them, and re-layouts  6.03 us (6%)
  between operations  1.29 us (1%)
    pallas_call x1, Pallas kernels, body(): pl.pallas_call(kernel, out_shape=(S((L, 128), BF), S((L, 128), BF), S((12...  99.9 us
    unnamed x10, local copies, waits for them, and re-layouts  4.84 us

profile of v1, /device:TPU:1, one launch (start us, length us, event | category | flops | bytes accessed | tf_op | source)
XLA Modules:
  0.0 107.2 jit_solution(1696999650398899368)
XLA Ops:
  1.3 99.9 %whole.1 = (bf16[2048,128]{1,0:T(8,128)(2,1)}, bf16[2048,128]{1,0:T(8,128)(2,1)}, bf16[128,2048]{1,0:T(8,128)(2,1)}, f32[16,2048]{1,0:T(8,128)}, f32[8,128]{1,0:T(8,128)}) custom-call(f32[1]{0:T(128)S(6)} %copy.15.lam_ref, bf16[128,2048]{1,0:T(8,128)(2,1)} %bitcast.8, bf16[128,2048]{1,0:T(8,128)(2,1)} %bitcast.9, bf16[16,2048]{1,0:T(8,128)(2,1)} %w_h.1, ...), custom_call_target="tpu_custom_call" | custom-call | tf_op jit(solution)/shard_map/whole/pallas_call | solution.py:495
  101.2 1.2 %slice.3 = f32[1,1]{1,0:T(1,128)} slice(f32[8,128]{1,0:T(8,128)} %get-tuple-element.14), slice={[0:1], [0:1]} | slice | bytes 8 | tf_op jit(solution)/shard_map/slice | solution.py:511
  102.4 0.0 copy-start.1
  102.4 1.9 %copy.16 = bf16[1,2048,1,128]{3,1,2,0:T(8,128)(2,1)} copy(bf16[1,2048,1,128]{3,1,2,0:T(8,128)(2,1)} %bitcast.14) | data formatting | bytes 1048576
  104.3 0.0 copy-done.1
  104.3 0.0 copy-start
  104.3 0.8 copy.17
  105.1 0.4 copy-done
  105.5 0.0 copy-start.2
  105.5 0.8 copy.18
  106.3 0.2 copy-done.2
  106.6 0.7 copy.19
Async XLA Ops:
  102.4 1.9 %copy-start.1 = (bf16[2048,128]{1,0:T(8,128)(2,1)S(1)}, bf16[2048,128]{1,0:T(8,128)(2,1)}, u32[]{:S(2)}) copy-start(bf16[2048,128]{1,0:T(8,128)(2,1)} %get-tuple-element.11) | copy-start | bytes 1572868
  104.3 1.2 %copy-start = (bf16[128,2048]{1,0:T(8,128)(2,1)S(1)}, bf16[128,2048]{1,0:T(8,128)(2,1)}, u32[]{:S(2)}) copy-start(bf16[128,2048]{1,0:T(8,128)(2,1)} %get-tuple-element.12) | copy-start | bytes 1572868
  105.5 1.0 copy-start.2

commit v2 on v1

--- a/solution.py
+++ b/solution.py
@@ -197,6 +197,40 @@
                 self.copy(k, slot, 0, 0, 0 if slot % 4 < 2 else 1, 0, 1).wait_send()
 
 
+class Ring:
+    def __init__(self, at, ss, rs, sp, dp, axis):
+        self.at, self.ss, self.rs, self.sp, self.dp, self.axis = at, ss, rs, sp, dp, axis
+
+    def index(self, o):
+        return lax.rem((lax.rem(self.sp, 4) if self.axis == 0 else lax.div(self.sp, 4)) + (o + 4), 4)
+
+    def copy(self, slot, o, part, delta):
+        i = self.index(delta)
+        to = lax.div(self.sp, 4) * 4 + i if self.axis == 0 else i * 4 + lax.rem(self.sp, 4)
+        ref = self.at(self.index(o), part)
+        return pltpu.make_async_remote_copy(
+            src_ref=ref, dst_ref=ref, send_sem=self.ss(slot), recv_sem=self.rs(slot),
+            device_id={"sp": to, "dp": self.dp}, device_id_type=MESH)
+
+    def start(self):
+        self.copy(0, 0, None, 1).start()
+        self.copy(1, 0, None, -1).start()
+
+    def near(self):
+        self.copy(0, -1, None, 1).wait_recv()
+        self.copy(2, -1, 0, 1).start()
+        self.copy(1, 1, None, -1).wait_recv()
+        self.copy(3, 1, 1, -1).start()
+
+    def far(self):
+        self.copy(2, 2, 0, 1).wait_recv()
+        self.copy(3, 2, 1, 1).wait_recv()
+
+    def drain(self):
+        for slot in range(4):
+            self.copy(slot, 0, None if slot < 2 else slot - 2, 1).wait_send()
+
+
 class Row:
     def __init__(self, w, ss, rs, sp, dp):
         self.w, self.ss, self.rs, self.sp, self.dp = w, ss, rs, sp, dp
@@ -233,9 +267,11 @@
         self.copy(3, 2, self.own(1), 1).wait_recv()
         self.other(7, 2).start()
 
-    def finish(self):
+    def arrived(self):
         for slot in (4, 5, 6, 7):
             self.other(slot, 0).wait_recv()
+
+    def drain(self):
         for slot in (0, 1, 4, 5, 6, 7):
             self.copy(slot, 0, self.own(1)).wait_send()
         for slot in (2, 3):
@@ -243,11 +279,14 @@
 
 
 def kernel(lam_ref, tok_h, cot_h, w_h, q_h, k_h, gq_h, gk_h, gt_h, gw_h, gl_h,
-           x, w, wh, cota, q_ref, k_ref, qz1, qz2, kt, vt, vn, s1, s2, p1, p2, aa, dot, do, delta, dqt, ot, o2t,
-           dvb, dvrow, gwt, gwp, gwin, gws, gwf, gqb, gkb, gtb, gwo, glb, glin,
-           load, save, xs, xr, ws, wr, rs_, rr, h1s, h1r, h2s, h2r, cs, cr, ds_, dr, es, er, ls, lr, fs, fr):
+           xr, xc, w, wo, wq, cota, q_ref, k_ref, qz1, qz2, kt, vt, vn, v4, s1, s2, p1, p2, aa, dot, do, delta, dqt, ot, o2t,
+           dvg, dvrow, gwt, gwp, gwin, gws, gwf, gqb, gkb, gtb, gwo, glb, glin,
+           load, wload, save, xs, xr_, ys, yr, zs, zr, ws, wr, rs_, rr, qs, qr, h1s, h1r, cs, cr, vs, vr, gs, gr, ds_, dr,
+           es, er, ls, lr, fs, fr):
     sp, dp = lax.axis_index("sp"), lax.axis_index("dp")
+    y, z = lax.rem(sp, 4), lax.div(sp, 4)
     lam = lam_ref[0]
+    scope = jax.named_scope
 
     def sp_peers(body):
         lax.fori_loop(1, 16, lambda d, c: (body(lax.rem(sp + d, 16)), c)[1], 0)
@@ -259,8 +298,8 @@
         return pltpu.make_async_remote_copy(src_ref=src, dst_ref=dst, send_sem=ss, recv_sem=rs,
                                             device_id={"sp": s, "dp": d}, device_id_type=MESH)
 
-    def lanes(h):
-        return pl.ds(pl.multiple_of(h * 128, 128), 128)
+    def lanes(h, n=128):
+        return pl.ds(pl.multiple_of(h * n, n), n)
 
     def rows(i, n=B):
         return pl.ds(pl.multiple_of(i * n, n), n)
@@ -269,23 +308,44 @@
     sp_peers(lambda s: pl.semaphore_signal(barrier, inc=1, device_id={"sp": s, "dp": dp}, device_id_type=MESH))
     dp_peers(lambda d: pl.semaphore_signal(barrier, inc=1, device_id={"sp": sp, "dp": d}, device_id_type=MESH))
     loads = [pltpu.make_async_copy(a, b, load.at[n]) for n, (a, b) in enumerate((
-        (w_h, w.at[sp, dp]), (tok_h, x.at[sp]), (q_h, q_ref), (k_h, k_ref), (cot_h.at[:, lanes(sp)], cota.at[rows(sp, 128)])))]
+        (w_h, w.at[sp, dp]), (tok_h, xr.at[y]), (q_h, q_ref), (k_h, k_ref), (cot_h.at[:, lanes(sp)], cota.at[rows(sp, 128)])))]
     for a in loads:
         a.start()
+    parts = [pltpu.make_async_copy(w_h.at[:, pl.ds((4 * b + a) * 128, 128)], wo.at[a, :, pl.ds(b * 128, 128)], wload.at[a, b])
+             for a in range(4) for b in range(4)]
+    for a in parts:
+        a.start()
+
+    def half_rows(ref):
+        return lambda i, part: ref.at[i] if part is None else ref.at[i, pl.ds(64 * part, 64)]
+
     wplane = Plane(lambda s, cols: w.at[s, dp, :, cols], ws, wr, sp, dp)
-    xplane = Plane(lambda s, cols: x.at[s, :, cols], xs, xr, sp, dp)
+    xring = Ring(half_rows(xr), lambda n: xs.at[n], lambda n: xr_.at[n], sp, dp, 0)
+    cring = Ring(lambda i, part: xc.at[i] if part is None else xc.at[i, pl.ds(2 * part, 2)],
+                 lambda n: ys.at[n], lambda n: yr.at[n], sp, dp, 0)
     wrow = Row(w, rs_, rr, sp, dp)
-    loads[0].wait()
-    wh[sp, dp] = w[sp, dp, :, lanes(sp)]
-    loads[1].wait()
-    pl.semaphore_wait(barrier, 22)
+    qrow = Row(wq, qs, qr, sp, dp)
+    for a in parts + loads[:2]:
+        a.wait()
+    wq[sp, dp] = wo[y]
+    xc[y, z] = xr[y, :, lanes(z, 512)]
+    with scope("barrier"):
+        pl.semaphore_wait(barrier, 22)
+
+    def head_rows(s, src, to):
+        return remote(wo.at[lax.rem(to, 4)], wq.at[src, dp], h1s.at[to], h1r.at[src], s, dp)
+
+    def columns(zz, src, to):
+        return remote(xr.at[y, :, lanes(to, 512)], xc.at[y, src], zs.at[to], zr.at[src], zz * 4 + y, dp)
+
+    def z_peers(body):
+        for d in (1, 3, 2):
+            body(lax.rem(z + d, 4))
 
     wplane.first()
-
-    def part_of(s, src, dst):
-        return remote(w.at[sp, dp, :, lanes(src)], wh.at[dst, dp], h1s.at[src], h1r.at[dst], s, dp)
-    sp_peers(lambda s: part_of(s, s, sp).start())
-    xplane.first()
+    sp_peers(lambda s: head_rows(s, sp, s).start())
+    xring.start()
+    z_peers(lambda t: columns(t, z, t).start())
     for k in (0, 1):
         wplane.second(k, 0)
     for n in (2, 3):
@@ -303,71 +363,96 @@
     def soft(lo, hi):
         lax.fori_loop(lo, hi, lambda i, c: (softmaxes(i, lam, k_ref, qz1, qz2, s1, s2, p1, p2, aa), c)[1], 0)
 
-    wplane.near()
-    for k in (0, 1):
-        xplane.second(k, 0)
-
-    sp_peers(lambda s: part_of(s, sp, s).wait_recv())
-
-    def column(d, src):
-        return remote(wh.at[:, src], wh.at[:, src], h2s.at[d], h2r.at[src], sp, d)
-    dp_peers(lambda d: column(d, dp).start())
-    soft(0, 3)
-    for n in (0,):
-        wplane.across(n)
-    wplane.far()
-    xplane.near()
-    soft(3, 5)
-    for n in (1, 2, 3):
-        wplane.across(n)
-    xplane.across(0)
-    xplane.far()
-    soft(5, 6)
-    for n in range(4):
-        wplane.last(n)
+    with scope("soft03"):
+        soft(0, 3)
+    with scope("heads"):
+        sp_peers(lambda s: head_rows(s, s, sp).wait_recv())
+    qrow.start()
+    with scope("soft35"):
+        soft(3, 5)
+    with scope("wnear"):
+        wplane.near()
+    with scope("soft56"):
+        soft(5, 6)
+    with scope("qnear"):
+        qrow.near()
+    with scope("xnear"):
+        xring.near()
+
+    def cot_part(s, src, to):
+        return remote(cot_h.at[:, lanes(to)], cota.at[rows(src, 128)], cs.at[to], cr.at[src], s, dp)
+    sp_peers(lambda s: cot_part(s, sp, s).start())
+    with scope("soft67"):
+        soft(6, 7)
+    with scope("qfar"):
+        qrow.far()
+    with scope("soft78"):
+        soft(7, 8)
+    with scope("wacross0"):
+        wplane.across(0)
+    with scope("wfar"):
+        wplane.far()
+    with scope("qall"):
+        qrow.arrived()
+    with scope("xfar"):
+        xring.far()
+
+    def v_part(zz, src, to):
+        return remote(v4.at[to], vn.at[pl.ds(2 * src, 2)], vs.at[to], vr.at[src], zz * 4 + y, dp)
+
+    with scope("values"):
+        for n in (0, 1):
+            v = nn(xr[...].reshape(512, 2048), wq[:, :, :, n * 256:(n + 1) * 256].reshape(2048, 256)).astype(BF)
+            for m in (0, 1):
+                t = 2 * n + m
+                v4[t] = v[:, m * 128:(m + 1) * 128].reshape(2, B, 128)
+
+                @pl.when(t != z)
+                def _():
+                    v_part(t, z, t).start()
+        vn[pl.ds(2 * z, 2)] = v4[z]
+    with scope("columns"):
+        z_peers(lambda t: columns(t, t, z).wait_recv())
+    cring.start()
+
+    def mixed(r):
+        def one(e, c):
+            j = 2 * r + e
+            v = vn[j].T
+            vt[j] = v
+
+            def add(i, count):
+                for m in range(count):
+                    t = tri(i + m, j)
+                    ot[i + m] += nn(v, aa[t])
+                    o2t[i + m] += nn(v, p2[t])
+            paired(j, NB - j, add)
+            return c
+        lax.fori_loop(0, 2, one, 0)
+
+    with scope("mix0"):
+        mixed(z)
+    with scope("wacross"):
+        for n in (1, 2, 3):
+            wplane.across(n)
+    for d in (1, 3):
+        t = lax.rem(z + d, 4)
+        with scope("v%d" % d):
+            v_part(t, t, z).wait_recv()
+        with scope("mix%d" % d):
+            mixed(t)
+    with scope("wlast"):
+        for n in range(4):
+            wplane.last(n)
     wrow.start()
-    soft(6, 8)
-    dp_peers(lambda d: column(dp, d).wait_recv())
-
-    def values(j):
-        v = nn(x[pl.ds(2 * j, 2)].reshape(B, 2048), wh[...].reshape(2048, 128)).astype(BF)
-        vn[j] = v
-        v = v.T
-        vt[j] = v
-
-        def add(i, count):
-            for m in range(count):
-                t = tri(i + m, j)
-                ot[i + m] += nn(v, aa[t])
-                o2t[i + m] += nn(v, p2[t])
-        paired(j, NB - j, add)
-
-    y, z = lax.rem(sp, 4), lax.div(sp, 4)
-    side = lax.div(y, 2)
-
-    def pair(dz, which):
-        return 2 * lax.rem(z + dz, 4) + (side if which == 0 else 1 - side)
-    many = lambda js: lax.fori_loop(0, len(js), lambda n, c: (values(sum(jnp.where(n == m, j, 0) for m, j in enumerate(js))), c)[1], 0)
-
-    many([pair(0, 0)])
-    xplane.across(1)
-    xplane.across(2)
-    many([pair(1, 0), pair(3, 0)])
-    xplane.last(0)
-    many([pair(0, 1)])
-    xplane.across(3)
-
-    def cot_part(s, src, dst):
-        return remote(cot_h.at[:, lanes(src)], cota.at[rows(dst, 128)], cs.at[src], cr.at[dst], s, dp)
-    sp_peers(lambda s: cot_part(s, s, sp).start())
-    xplane.last(1)
-    xplane.last(2)
-    many([pair(1, 1), pair(3, 1), pair(2, 0)])
-    xplane.last(3)
-    many([pair(2, 1)])
-    wrow.near()
-    loads[4].wait()
-    sp_peers(lambda s: cot_part(s, sp, s).wait_recv())
+    t = lax.rem(z + 2, 4)
+    with scope("v2"):
+        v_part(t, t, z).wait_recv()
+    with scope("mix2"):
+        mixed(t)
+    with scope("cot"):
+        loads[4].wait()
+        sp_peers(lambda s: cot_part(s, s, sp).wait_recv())
 
     def mix(i, total):
         o, o2 = ot[i], o2t[i]
@@ -383,107 +468,169 @@
         delta[i, 0:1, :] = d1
         delta[i, 1:2, :] = d2
         return total + d2
-    total = lax.fori_loop(0, NB, mix, jnp.zeros((1, B), F32))
+    with scope("mix"):
+        total = lax.fori_loop(0, NB, mix, jnp.zeros((1, B), F32))
     glb[...] = jnp.broadcast_to(-jnp.sum(total, axis=1, keepdims=True), (8, 128))
-    gwt[...] = jnp.zeros_like(gwt)
 
     half = lax.broadcasted_iota(jnp.int32, (1, 128), 1) < 64
     ks = jnp.where(half, SCALE, -lam * SCALE)
 
-    def dv_part(s, t, src):
-        return remote(dvb.at[t], dvrow.at[:, lanes(src)], ds_.at[t], dr.at[src], s, dp)
-
-    def main(j, c):
+    def gl_part(d, src, to):
+        return remote(glb, glin.at[src], ls.at[to], lr.at[src], sp, d)
+
+    def dv_part(s, src, to):
+        j = lax.div(to, 2)
+        return remote(dvg.at[z, j, rows(lax.rem(to, 2), 128)], dvrow.at[:, lanes(src)], ds_.at[to], dr.at[src], s, dp)
+
+    def dv_ring(j):
+        return Ring(lambda i, part: dvg.at[i, j] if part is None else dvg.at[i, j, pl.ds(128 * part, 128)],
+                    lambda n: gs.at[j, n], lambda n: gr.at[j, n], sp, dp, 1)
+
+    def main(n, c):
+        j = NB - 1 - n
         dv, dk1, dk2 = keys_block(j, vn, qz1, qz2, kt, p1, p2, aa, dot, do, delta, dqt)
+        dvg[z, j] = dv.astype(BF)
         gkb[rows(j), :] = ((dk1 + dk2) * ks).astype(BF)
-        dvt = dv.T.astype(BF)
-        dvl = dv.astype(BF)
-        dvb[2 * j] = dvl[:128]
-        dvb[2 * j + 1] = dvl[128:]
-        for n in range(4):
-            cols = pl.ds(n * 512, 512)
-            gwt[:, cols] += nn(dvt, x[pl.ds(2 * j, 2), :, cols].reshape(B, 512))
+        dv_ring(j).start()
         for e in range(2):
             t = 2 * j + e
 
             @pl.when(t != sp)
             def _():
-                dv_part(t, t, sp).start()
-        return c
-    lax.fori_loop(0, NB, main, 0)
-    dvrow[:, lanes(sp)] = dvb[sp]
+                dv_part(t, sp, t).start()
+
+        @pl.when(n >= 4)
+        def _():
+            dv_ring(j + 4).near()
+        return c
+    with scope("cnear"):
+        cring.near()
+    with scope("main"):
+        lax.fori_loop(0, NB, main, 0)
+    save_k = pltpu.make_async_copy(gkb, gk_h, save.at[0])
+    save_k.start()
+
+    def fin(i, c):
+        gqb[rows(i), :] = (dqt[i].T * ks).astype(BF)
+        return c
+    with scope("fin"):
+        lax.fori_loop(0, NB, fin, 0)
+    save_q = pltpu.make_async_copy(gqb, gq_h, save.at[1])
+    save_q.start()
+    dvrow[:, lanes(sp)] = dvg[z, lax.div(sp, 2), rows(lax.rem(sp, 2), 128), :]
+    gwt[...] = jnp.zeros_like(gwt)
+
+    def weight_part(h, j):
+        jz, jy = lax.div(j, 2), lax.rem(j, 2)
+        cols = xc[pl.ds(2 * jy, 2), jz].reshape(B, 512)
+        gwt[h] += nn(dvg[h, j].T, cols)
+
+    def pieces(lo, hi, offsets):
+        def one(j, c):
+            for o in offsets:
+                weight_part(lax.rem(z + o, 4), j)
+            return c
+        lax.fori_loop(lo, hi, one, 0)
+
+    with scope("cfar"):
+        cring.far()
+    with scope("pieces0"):
+        pieces(0, 8, (0,))
+    with scope("pieces13"):
+        pieces(4, 8, (1, 3))
+
+    def late(n, c):
+        j = 3 - n
+        dv_ring(j).near()
+        weight_part(lax.rem(z + 1, 4), j)
+        weight_part(lax.rem(z + 3, 4), j)
+        return c
+    with scope("late"):
+        lax.fori_loop(0, 4, late, 0)
+
+    def distant(n, c):
+        dv_ring(7 - n).far()
+        weight_part(lax.rem(z + 2, 4), 7 - n)
+        return c
+    with scope("distant"):
+        lax.fori_loop(0, 8, distant, 0)
 
     def out_rows(n, c):
-        part = gwt[:, rows(n, 128)].T.astype(BF)
-        gwp[n] = part.reshape(8, 16, 128)
-        return c
-    lax.fori_loop(0, 16, out_rows, 0)
-
-    def gw_part(d, to, src):
+        for h in range(4):
+            gwp[n, :, :, h * 128:(h + 1) * 128] = gwt[h, :, rows(n, 128)].T.astype(BF).reshape(8, 16, 128)
+        return c
+    with scope("outrows"):
+        lax.fori_loop(0, 4, out_rows, 0)
+
+    def gw_part(d, src, to):
         return remote(gwp.at[:, to], gwin.at[src], es.at[to], er.at[src], sp, d)
-
-    def gl_part(d, to, src):
-        return remote(glb, glin.at[src], ls.at[to], lr.at[src], sp, d)
-    dp_peers(lambda d: gw_part(d, d, dp).start())
-    dp_peers(lambda d: gl_part(d, d, dp).start())
+    dp_peers(lambda d: gw_part(d, dp, d).start())
+    dp_peers(lambda d: gl_part(d, dp, d).start())
     gwin[dp] = gwp[:, dp]
     glin[dp] = glb[...]
-
-    save_k = pltpu.make_async_copy(gkb, gk_h, save.at[0])
-    save_k.start()
-    wrow.far()
-
-    def fin(i, c):
-        gqb[rows(i), :] = (dqt[i].T * ks).astype(BF)
-        return c
-    lax.fori_loop(0, NB, fin, 0)
-    save_q = pltpu.make_async_copy(gqb, gq_h, save.at[1])
-    save_q.start()
-    sp_peers(lambda s: dv_part(s, s, s).wait_recv())
-    wrow.finish()
-
-    def tokens_grad(n, c):
-        g = nt(dvrow[...], w[pl.ds(2 * n, 2)].reshape(B, 2048))
-        gtb[:, rows(n)] = g.astype(BF)
-        return c
-    lax.fori_loop(0, NB, tokens_grad, 0)
-    save_t = pltpu.make_async_copy(gtb, gt_h, save.at[2])
-    save_t.start()
-
-    dp_peers(lambda d: gw_part(d, d, d).wait_recv())
+    with scope("wrownear"):
+        wrow.near()
+    with scope("dvwait"):
+        sp_peers(lambda s: dv_part(s, s, sp).wait_recv())
+    with scope("wrowfar"):
+        wrow.far()
+    with scope("gwwait"):
+        dp_peers(lambda d: gw_part(d, d, dp).wait_recv())
     acc = gwin[0].astype(F32)
     for d in range(1, 8):
         acc = acc + gwin[d].astype(F32)
     gws[...] = acc.astype(BF)
 
-    def fin_part(s, to, src):
-        return remote(gws.at[to], gwf.at[src], fs.at[to], fr.at[src], s, dp)
-    sp_peers(lambda s: fin_part(s, s, sp).start())
-    gwf[sp] = gws[sp]
-    dp_peers(lambda d: gl_part(d, d, d).wait_recv())
+    def y_peers(body):
+        for d in (1, 3, 2):
+            body(lax.rem(y + d, 4))
+
+    def fin_part(yy, src, to):
+        return remote(gws.at[to], gwf.at[src], fs.at[to], fr.at[src], z * 4 + yy, dp)
+    y_peers(lambda t: fin_part(t, y, t).start())
+    gwf[y] = gws[y]
+    dp_peers(lambda d: gl_part(d, d, dp).wait_recv())
     tot = glin[0]
     for d in range(1, 8):
         tot = tot + glin[d]
-    glb2 = delta
-    glb2[0] = jnp.concatenate([tot, tot], axis=1)
-    save_l = pltpu.make_async_copy(glb2.at[0, :, pl.ds(0, 128)], gl_h, save.at[3])
+    delta[0] = jnp.concatenate([tot, tot], axis=1)
+    save_l = pltpu.make_async_copy(delta.at[0, :, pl.ds(0, 128)], gl_h, save.at[3])
     save_l.start()
-    xplane.drain()
-    wplane.drain()
-    sp_peers(lambda s: part_of(s, s, sp).wait_send())
-    dp_peers(lambda d: column(d, dp).wait_send())
-    sp_peers(lambda s: cot_part(s, s, sp).wait_send())
-    sp_peers(lambda s: dv_part(s, s, sp).wait_send())
-    dp_peers(lambda d: gw_part(d, d, dp).wait_send())
-    dp_peers(lambda d: gl_part(d, d, dp).wait_send())
-    sp_peers(lambda s: fin_part(s, s, s).wait_recv())
-    for h in range(16):
-        gwo[:, h * 128:(h + 1) * 128] = gwf[h].astype(F32)
+    with scope("wrowall"):
+        wrow.arrived()
+
+    def tokens_grad(n, c):
+        g = nt(dvrow[...], w[pl.ds(2 * n, 2)].reshape(B, 2048))
+        gtb[:, rows(n)] = g.astype(BF)
+        return c
+    with scope("tgrad"):
+        lax.fori_loop(0, NB, tokens_grad, 0)
+    save_t = pltpu.make_async_copy(gtb, gt_h, save.at[2])
+    save_t.start()
+    with scope("finwait"):
+        y_peers(lambda t: fin_part(t, t, y).wait_recv())
+    for a in range(4):
+        for b in range(4):
+            gwo[:, (4 * b + a) * 128:(4 * b + a + 1) * 128] = gwf[a, :, b * 128:(b + 1) * 128].astype(F32)
     save_w = pltpu.make_async_copy(gwo, gw_h, save.at[4])
     save_w.start()
-    sp_peers(lambda s: fin_part(s, s, sp).wait_send())
-    for a in (save_k, save_q, save_t, save_l, save_w):
-        a.wait()
+    xring.drain()
+    cring.drain()
+    wplane.drain()
+    wrow.drain()
+    qrow.drain()
+    lax.fori_loop(0, NB, lambda j, c: (dv_ring(j).drain(), c)[1], 0)
+    sp_peers(lambda s: head_rows(s, sp, s).wait_send())
+    sp_peers(lambda s: cot_part(s, sp, s).wait_send())
+    sp_peers(lambda s: dv_part(s, sp, s).wait_send())
+    z_peers(lambda t: columns(t, z, t).wait_send())
+    z_peers(lambda t: v_part(t, z, t).wait_send())
+    dp_peers(lambda d: gw_part(d, dp, d).wait_send())
+    dp_peers(lambda d: gl_part(d, dp, d).wait_send())
+    y_peers(lambda t: fin_part(t, y, t).wait_send())
+    with scope("savewait"):
+        for a in (save_k, save_q, save_t, save_l, save_w):
+            a.wait()
 
 
 def body(tokens, cotangent, value_weight, query_heads, key_heads, lambdas):
@@ -497,15 +644,17 @@
         out_shape=(S((L, 128), BF), S((L, 128), BF), S((128, 2048), BF), S((16, 2048), F32), S((8, 128), F32)),
         in_specs=[smem] + [anywhere] * 5, out_specs=[anywhere] * 5,
         scratch_shapes=[
-            V((16, 128, 2048), BF), V((16, 8, 16, 2048), BF), V((16, 8, 16, 128), BF), V((L, 128), BF), V((L, 128), BF), V((L, 128), BF),
-            V((NB, B, 128), BF), V((NB, B, 128), BF), V((NB, 128, B), BF), V((NB, 128, B), BF), V((NB, B, 128), BF),
+            V((4, 128, 2048), BF), V((4, 4, 128, 512), BF), V((16, 8, 16, 2048), BF), V((4, 16, 512), BF), V((16, 8, 16, 512), BF),
+            V((L, 128), BF), V((L, 128), BF), V((L, 128), BF),
+            V((NB, B, 128), BF), V((NB, B, 128), BF), V((NB, 128, B), BF), V((NB, 128, B), BF), V((NB, B, 128), BF), V((4, 2, B, 128), BF),
             V((NB, B, B), F32), V((NB, B, B), F32), V(tiles, BF), V(tiles, BF), V(tiles, BF),
             V((NB, 128, B), BF), V((NB, B, 128), BF), V((NB, 8, B), F32), V((NB, 128, B), F32), V((NB, 128, B), F32), V((NB, 128, B), F32),
-            V((16, 128, 128), BF), V((128, 2048), BF), V((128, 2048), F32), V((16, 8, 16, 128), BF), V((8, 16, 16, 128), BF),
-            V((16, 16, 128), BF), V((16, 16, 128), BF), V((L, 128), BF), V((L, 128), BF), V((128, 2048), BF), V((16, 2048), F32),
+            V((4, NB, B, 128), BF), V((128, 2048), BF), V((4, 128, 512), F32), V((4, 8, 16, 512), BF), V((8, 4, 16, 512), BF),
+            V((4, 16, 512), BF), V((4, 16, 512), BF), V((L, 128), BF), V((L, 128), BF), V((128, 2048), BF), V((16, 2048), F32),
             V((8, 128), F32), V((8, 8, 128), F32),
-            dma(5), dma(5), dma(2, 20), dma(2, 20), dma(2, 20), dma(2, 20), dma(8), dma(8), dma(16), dma(16), dma(8), dma(8),
-            dma(16), dma(16), dma(16), dma(16), dma(8), dma(8), dma(8), dma(8), dma(16), dma(16)],
+            dma(5), dma(4, 4), dma(5), dma(4), dma(4), dma(4), dma(4), dma(4), dma(4), dma(2, 20), dma(2, 20), dma(8), dma(8), dma(8), dma(8),
+            dma(16), dma(16), dma(16), dma(16), dma(4), dma(4), dma(8, 4), dma(8, 4), dma(16), dma(16),
+            dma(8), dma(8), dma(8), dma(8), dma(4), dma(4)],
         compiler_params=pltpu.CompilerParams(vmem_limit_bytes=60 * 1024 * 1024, collective_id=0, has_side_effects=True),
         name="whole")(lambdas, tokens[0], cotangent[0], value_weight, query_heads.reshape(L, 128), key_heads.reshape(L, 128))
     return gq.reshape(query_heads.shape), gk.reshape(key_heads.shape), gt[None], gw, gl[0, 0:1]

time: 109 us -> 118 us (1.083)
  Pallas kernels: 99.9 us -> 110 us
    pallas_call x1, Pallas kernels: 99.9 us -> 110 us  [body(): pl.pallas_call(kernel, out_shape=(S((L, 128), BF), S((L, 128), BF), S((12...]
where the time goes in v2:
time: 118 us; the launch traced here: 117 us
  Pallas kernels  110 us (93%)
  local copies, waits for them, and re-layouts  6.03 us (5%)
  between operations  1.29 us (1%)
    pallas_call x1, Pallas kernels, body(): pl.pallas_call(kernel, out_shape=(S((L, 128), BF), S((L, 128), BF), S((12...  110 us
    unnamed x10, local copies, waits for them, and re-layouts  4.84 us

profile of v2, /device:TPU:1, one launch (start us, length us, event | category | flops | bytes accessed | tf_op | source)
XLA Modules:
  0.0 117.2 jit_solution(6019080269832995343)
XLA Ops:
  1.3 109.9 %whole.1 = (bf16[2048,128]{1,0:T(8,128)(2,1)}, bf16[2048,128]{1,0:T(8,128)(2,1)}, bf16[128,2048]{1,0:T(8,128)(2,1)}, f32[16,2048]{1,0:T(8,128)}, f32[8,128]{1,0:T(8,128)}) custom-call(f32[1]{0:T(128)S(6)} %copy.15.lam_ref, bf16[128,2048]{1,0:T(8,128)(2,1)} %bitcast.8, bf16[128,2048]{1,0:T(8,128)(2,1)} %bitcast.9, bf16[16,2048]{1,0:T(8,128)(2,1)} %w_h.1, ...), custom_call_target="tpu_custom_call" | custom-call | tf_op jit(solution)/shard_map/whole/pallas_call | solution.py:642
  111.2 1.2 %slice.3 = f32[1,1]{1,0:T(1,128)} slice(f32[8,128]{1,0:T(8,128)} %get-tuple-element.14), slice={[0:1], [0:1]} | slice | bytes 8 | tf_op jit(solution)/shard_map/slice | solution.py:660
  112.4 0.0 copy-start.1
  112.4 1.9 %copy.16 = bf16[1,2048,1,128]{3,1,2,0:T(8,128)(2,1)} copy(bf16[1,2048,1,128]{3,1,2,0:T(8,128)(2,1)} %bitcast.14) | data formatting | bytes 1048576
  114.3 0.0 copy-done.1
  114.3 0.0 copy-start
  114.3 0.8 copy.17
  115.1 0.4 copy-done
  115.6 0.0 copy-start.2
  115.6 0.8 copy.18
  116.4 0.2 copy-done.2
  116.6 0.7 copy.19
Async XLA Ops:
  112.4 1.9 %copy-start.1 = (bf16[2048,128]{1,0:T(8,128)(2,1)S(1)}, bf16[2048,128]{1,0:T(8,128)(2,1)}, u32[]{:S(2)}) copy-start(bf16[2048,128]{1,0:T(8,128)(2,1)} %get-tuple-element.11) | copy-start | bytes 1572868
  114.3 1.2 %copy-start = (bf16[128,2048]{1,0:T(8,128)(2,1)S(1)}, bf16[128,2048]{1,0:T(8,128)(2,1)}, u32[]{:S(2)}) copy-start(bf16[128,2048]{1,0:T(8,128)(2,1)} %get-tuple-element.12) | copy-start | bytes 1572868
  115.6 1.0 copy-start.2

commit v3 on v2

--- a/solution.py
+++ b/solution.py
@@ -132,71 +132,6 @@
 S = jax.ShapeDtypeStruct
 
 
-class Plane:
-    def __init__(self, at, ss, rs, sp, dp):
-        self.at, self.ss, self.rs, self.dp = at, ss, rs, dp
-        self.pos = (lax.rem(sp, 4), lax.div(sp, 4))
-
-    def block(self, k, o, p):
-        a = lax.rem(self.pos[k] + (o + 4), 4)
-        b = lax.rem(self.pos[1 - k] + (p + 4), 4)
-        return b * 4 + a if k == 0 else a * 4 + b
-
-    def copy(self, k, slot, o, p, part, axis, delta):
-        s = self.block(k, o, p)
-        cols = pl.ds(k * 1024 + (512 if part == 2 else 0), 1024 if part == 0 else 512)
-        to = self.block(0, delta, 0) if axis == 0 else self.block(0, 0, delta)
-        return pltpu.make_async_remote_copy(
-            src_ref=self.at(s, cols), dst_ref=self.at(s, cols), send_sem=self.ss.at[k, slot], recv_sem=self.rs.at[k, slot],
-            device_id={"sp": to, "dp": self.dp}, device_id_type=MESH)
-
-    def first(self):
-        for k in (0, 1):
-            self.copy(k, 0, 0, 0, 0, k, 1).start()
-            self.copy(k, 1, 0, 0, 0, k, -1).start()
-
-    def second(self, k, n):
-        o = (0, -1, 1, 2)[n]
-        self.copy(k, 4 + 4 * n, o, 0, 0, 1 - k, 1).start()
-        self.copy(k, 5 + 4 * n, o, 0, 0, 1 - k, -1).start()
-
-    def near(self):
-        for k in (0, 1):
-            self.copy(k, 0, -1, 0, 0, k, 1).wait_recv()
-            self.copy(k, 2, -1, 0, 1, k, 1).start()
-            self.copy(k, 1, 1, 0, 0, k, -1).wait_recv()
-            self.copy(k, 3, 1, 0, 2, k, -1).start()
-        for k in (0, 1):
-            self.second(k, 1)
-        for k in (0, 1):
-            self.second(k, 2)
-
-    def far(self):
-        for k in (0, 1):
-            self.copy(k, 2, 2, 0, 1, k, 1).wait_recv()
-            self.copy(k, 3, 2, 0, 2, k, 1).wait_recv()
-            self.second(k, 3)
-
-    def across(self, n):
-        o = (0, -1, 1, 2)[n]
-        for k in (0, 1):
-            self.copy(k, 4 + 4 * n, o, -1, 0, 1 - k, 1).wait_recv()
-            self.copy(k, 6 + 4 * n, o, -1, 1, 1 - k, 1).start()
-            self.copy(k, 5 + 4 * n, o, 1, 0, 1 - k, -1).wait_recv()
-            self.copy(k, 7 + 4 * n, o, 1, 2, 1 - k, -1).start()
-
-    def last(self, n):
-        o = (0, -1, 1, 2)[n]
-        for k in (0, 1):
-            self.copy(k, 6 + 4 * n, o, 2, 1, 1 - k, 1).wait_recv()
-            self.copy(k, 7 + 4 * n, o, 2, 2, 1 - k, 1).wait_recv()
-
-    def drain(self):
-        for k in (0, 1):
-            for slot in range(20):
-                self.copy(k, slot, 0, 0, 0 if slot % 4 < 2 else 1, 0, 1).wait_send()
-
-
 class Ring:
     def __init__(self, at, ss, rs, sp, dp, axis):
         self.at, self.ss, self.rs, self.sp, self.dp, self.axis = at, ss, rs, sp, dp, axis
@@ -231,6 +166,30 @@
             self.copy(slot, 0, None if slot < 2 else slot - 2, 1).wait_send()
 
 
+class SplitRing(Ring):
+    def start(self, n):
+        self.copy(2 * n, 0, n, 1).start()
+        self.copy(2 * n + 1, 0, n, -1).start()
+
+    def near(self, n):
+        if n == 0:
+            self.copy(0, -1, 0, 1).wait_recv()
+            self.copy(4, -1, 0, 1).start()
+            self.copy(1, 1, 0, -1).wait_recv()
+        else:
+            self.copy(3, 1, 1, -1).wait_recv()
+            self.copy(5, 1, 1, -1).start()
+            self.copy(2, -1, 1, 1).wait_recv()
+
+    def far(self):
+        self.copy(4, 2, 0, 1).wait_recv()
+        self.copy(5, 2, 1, -1).wait_recv()
+
+    def drain(self):
+        for slot, n in enumerate((0, 0, 1, 1, 0, 1)):
+            self.copy(slot, 0, n, 1).wait_send()
+
+
 class Row:
     def __init__(self, w, ss, rs, sp, dp):
         self.w, self.ss, self.rs, self.sp, self.dp = w, ss, rs, sp, dp
@@ -280,7 +239,7 @@
 
 def kernel(lam_ref, tok_h, cot_h, w_h, q_h, k_h, gq_h, gk_h, gt_h, gw_h, gl_h,
            xr, xc, w, wo, wq, cota, q_ref, k_ref, qz1, qz2, kt, vt, vn, v4, s1, s2, p1, p2, aa, dot, do, delta, dqt, ot, o2t,
-           dvg, dvrow, gwt, gwp, gwin, gws, gwf, gqb, gkb, gtb, gwo, glb, glin,
+           dvg, dvin, dvrow, gwt, gwp, gwin, gws, gwf, gqb, gkb, gtb, gwo, glb, glin,
            load, wload, save, xs, xr_, ys, yr, zs, zr, ws, wr, rs_, rr, qs, qr, h1s, h1r, cs, cr, vs, vr, gs, gr, ds_, dr,
            es, er, ls, lr, fs, fr):
     sp, dp = lax.axis_index("sp"), lax.axis_index("dp")
@@ -297,6 +256,9 @@
     def remote(src, dst, ss, rs, s, d):
         return pltpu.make_async_remote_copy(src_ref=src, dst_ref=dst, send_sem=ss, recv_sem=rs,
                                             device_id={"sp": s, "dp": d}, device_id_type=MESH)
+
+    def all_of(ref, sem):
+        pltpu.make_async_copy(ref, ref, sem.at[0]).wait()
 
     def lanes(h, n=128):
         return pl.ds(pl.multiple_of(h * n, n), n)
@@ -311,7 +273,7 @@
         (w_h, w.at[sp, dp]), (tok_h, xr.at[y]), (q_h, q_ref), (k_h, k_ref), (cot_h.at[:, lanes(sp)], cota.at[rows(sp, 128)])))]
     for a in loads:
         a.start()
-    parts = [pltpu.make_async_copy(w_h.at[:, pl.ds((4 * b + a) * 128, 128)], wo.at[a, :, pl.ds(b * 128, 128)], wload.at[a, b])
+    parts = [pltpu.make_async_copy(w_h.at[:, pl.ds((4 * b + a) * 128, 128)], wo.at[a, :, pl.ds(b * 128, 128)], wload.at[0])
              for a in range(4) for b in range(4)]
     for a in parts:
         a.start()
@@ -319,35 +281,40 @@
     def half_rows(ref):
         return lambda i, part: ref.at[i] if part is None else ref.at[i, pl.ds(64 * part, 64)]
 
-    wplane = Plane(lambda s, cols: w.at[s, dp, :, cols], ws, wr, sp, dp)
-    xring = Ring(half_rows(xr), lambda n: xs.at[n], lambda n: xr_.at[n], sp, dp, 0)
+    wy = Ring(lambda i, part: w.at[z * 4 + i, dp] if part is None else w.at[z * 4 + i, dp, :, pl.ds(1024 * part, 1024)],
+              lambda n: ws.at[0, n], lambda n: wr.at[0, n], sp, dp, 0)
+    wz = Ring(lambda i, part: w.at[pl.ds(4 * i, 4), dp] if part is None else w.at[pl.ds(4 * i + 2 * part, 2), dp],
+              lambda n: ws.at[1, n], lambda n: wr.at[1, n], sp, dp, 1)
+    xring = SplitRing(half_rows(xr), lambda n: xs.at[n], lambda n: xr_.at[n], sp, dp, 0)
     cring = Ring(lambda i, part: xc.at[i] if part is None else xc.at[i, pl.ds(2 * part, 2)],
                  lambda n: ys.at[n], lambda n: yr.at[n], sp, dp, 0)
     wrow = Row(w, rs_, rr, sp, dp)
     qrow = Row(wq, qs, qr, sp, dp)
-    for a in parts + loads[:2]:
+    for a in loads[:2]:
         a.wait()
+    all_of(wo, wload)
     wq[sp, dp] = wo[y]
     xc[y, z] = xr[y, :, lanes(z, 512)]
     with scope("barrier"):
         pl.semaphore_wait(barrier, 22)
 
     def head_rows(s, src, to):
-        return remote(wo.at[lax.rem(to, 4)], wq.at[src, dp], h1s.at[to], h1r.at[src], s, dp)
+        return remote(wo.at[lax.rem(to, 4)], wq.at[src, dp], h1s.at[0], h1r.at[0], s, dp)
 
     def columns(zz, src, to):
-        return remote(xr.at[y, :, lanes(to, 512)], xc.at[y, src], zs.at[to], zr.at[src], zz * 4 + y, dp)
+        return remote(xr.at[y, :, lanes(to, 512)], xc.at[y, src], zs.at[0], zr.at[0], zz * 4 + y, dp)
 
     def z_peers(body):
         for d in (1, 3, 2):
             body(lax.rem(z + d, 4))
 
-    wplane.first()
     sp_peers(lambda s: head_rows(s, sp, s).start())
-    xring.start()
+    wy.start()
+    xring.start(0)
     z_peers(lambda t: columns(t, z, t).start())
-    for k in (0, 1):
-        wplane.second(k, 0)
+    def cot_part(s, src, to):
+        return remote(cot_h.at[:, lanes(to)], cota.at[rows(src, 128)], cs.at[0], cr.at[0], s, dp)
+
     for n in (2, 3):
         loads[n].wait()
 
@@ -366,39 +333,43 @@
     with scope("soft03"):
         soft(0, 3)
     with scope("heads"):
-        sp_peers(lambda s: head_rows(s, s, sp).wait_recv())
+        all_of(wq.at[pl.ds(0, 15), 0], h1r)
     qrow.start()
+    with scope("wynear"):
+        wy.near()
+    xring.start(1)
     with scope("soft35"):
         soft(3, 5)
-    with scope("wnear"):
-        wplane.near()
+    with scope("xnear0"):
+        xring.near(0)
     with scope("soft56"):
         soft(5, 6)
+    with scope("wyfar"):
+        wy.far()
+    wz.start()
+    with scope("soft67"):
+        soft(6, 7)
     with scope("qnear"):
         qrow.near()
-    with scope("xnear"):
-        xring.near()
-
-    def cot_part(s, src, to):
-        return remote(cot_h.at[:, lanes(to)], cota.at[rows(src, 128)], cs.at[to], cr.at[src], s, dp)
+    with scope("xnear1"):
+        xring.near(1)
     sp_peers(lambda s: cot_part(s, sp, s).start())
-    with scope("soft67"):
-        soft(6, 7)
+    with scope("columns"):
+        all_of(xc.at[0, pl.ds(0, 3)], zr)
+    cring.start()
+    with scope("soft78"):
+        soft(7, 8)
+    with scope("wznear"):
+        wz.near()
     with scope("qfar"):
         qrow.far()
-    with scope("soft78"):
-        soft(7, 8)
-    with scope("wacross0"):
-        wplane.across(0)
-    with scope("wfar"):
-        wplane.far()
     with scope("qall"):
         qrow.arrived()
     with scope("xfar"):
         xring.far()
 
     def v_part(zz, src, to):
-        return remote(v4.at[to], vn.at[pl.ds(2 * src, 2)], vs.at[to], vr.at[src], zz * 4 + y, dp)
+        return remote(v4.at[to], vn.at[pl.ds(2 * src, 2)], vs.at[0], vr.at[src], zz * 4 + y, dp)
 
     with scope("values"):
         for n in (0, 1):
@@ -411,9 +382,9 @@
                 def _():
                     v_part(t, z, t).start()
         vn[pl.ds(2 * z, 2)] = v4[z]
-    with scope("columns"):
-        z_peers(lambda t: columns(t, t, z).wait_recv())
-    cring.start()
+    with scope("wzfar"):
+        wz.far()
+    wrow.start()
 
     def mixed(r):
         def one(e, c):
@@ -432,19 +403,12 @@
 
     with scope("mix0"):
         mixed(z)
-    with scope("wacross"):
-        for n in (1, 2, 3):
-            wplane.across(n)
     for d in (1, 3):
         t = lax.rem(z + d, 4)
         with scope("v%d" % d):
             v_part(t, t, z).wait_recv()
         with scope("mix%d" % d):
             mixed(t)
-    with scope("wlast"):
-        for n in range(4):
-            wplane.last(n)
-    wrow.start()
     t = lax.rem(z + 2, 4)
     with scope("v2"):
         v_part(t, t, z).wait_recv()
@@ -452,7 +416,7 @@
         mixed(t)
     with scope("cot"):
         loads[4].wait()
-        sp_peers(lambda s: cot_part(s, s, sp).wait_recv())
+        all_of(cota.at[pl.ds(0, 1920)], cr)
 
     def mix(i, total):
         o, o2 = ot[i], o2t[i]
@@ -476,15 +440,31 @@
     ks = jnp.where(half, SCALE, -lam * SCALE)
 
     def gl_part(d, src, to):
-        return remote(glb, glin.at[src], ls.at[to], lr.at[src], sp, d)
-
-    def dv_part(s, src, to):
-        j = lax.div(to, 2)
-        return remote(dvg.at[z, j, rows(lax.rem(to, 2), 128)], dvrow.at[:, lanes(src)], ds_.at[to], dr.at[src], s, dp)
+        return remote(glb, glin.at[src], ls.at[0], lr.at[0], sp, d)
+
+    def dv_part(yy, src, to, h):
+        part = rows(lax.rem(to, 2), 128)
+        return remote(dvg.at[h, 2 * z + lax.div(to, 2), part], dvin.at[h, src], ds_.at[0], dr.at[0], z * 4 + yy, dp)
+
+    def y_peers(body):
+        for d in (1, 3, 2):
+            body(lax.rem(y + d, 4))
+
+    def gw_part(d, src, to, h):
+        return remote(gwp.at[h, to], gwin.at[h, src], es.at[0], er.at[0], sp, d)
+
+    def send_head(o, weights):
+        h = lax.rem(z + o, 4)
+        if weights:
+            for n in range(4):
+                gwp[h, :, n] = gwt[h, :, n * 128:(n + 1) * 128].T.astype(BF).reshape(8, 16, 128)
+            dp_peers(lambda d: gw_part(d, dp, d, h).start())
+        else:
+            y_peers(lambda t: dv_part(t, y, t, h).start())
 
     def dv_ring(j):
         return Ring(lambda i, part: dvg.at[i, j] if part is None else dvg.at[i, j, pl.ds(128 * part, 128)],
-                    lambda n: gs.at[j, n], lambda n: gr.at[j, n], sp, dp, 1)
+                    lambda n: gs.at[0], lambda n: gr.at[j, n], sp, dp, 1)
 
     def main(n, c):
         j = NB - 1 - n
@@ -492,21 +472,19 @@
         dvg[z, j] = dv.astype(BF)
         gkb[rows(j), :] = ((dk1 + dk2) * ks).astype(BF)
         dv_ring(j).start()
-        for e in range(2):
-            t = 2 * j + e
-
-            @pl.when(t != sp)
-            def _():
-                dv_part(t, sp, t).start()
-
-        @pl.when(n >= 4)
+
+        @pl.when(n >= 5)
         def _():
-            dv_ring(j + 4).near()
-        return c
-    with scope("cnear"):
-        cring.near()
+            dv_ring(j + 5).near()
+
+        @pl.when(n == 5)
+        def _():
+            cring.near()
+        return c
     with scope("main"):
         lax.fori_loop(0, NB, main, 0)
+    with scope("wrownear"):
+        wrow.near()
     save_k = pltpu.make_async_copy(gkb, gk_h, save.at[0])
     save_k.start()
 
@@ -517,7 +495,6 @@
         lax.fori_loop(0, NB, fin, 0)
     save_q = pltpu.make_async_copy(gqb, gq_h, save.at[1])
     save_q.start()
-    dvrow[:, lanes(sp)] = dvg[z, lax.div(sp, 2), rows(lax.rem(sp, 2), 128), :]
     gwt[...] = jnp.zeros_like(gwt)
 
     def weight_part(h, j):
@@ -534,19 +511,25 @@
 
     with scope("cfar"):
         cring.far()
+    send_head(0, False)
     with scope("pieces0"):
         pieces(0, 8, (0,))
+        send_head(0, True)
     with scope("pieces13"):
-        pieces(4, 8, (1, 3))
+        pieces(5, 8, (1, 3))
 
     def late(n, c):
-        j = 3 - n
+        j = 4 - n
         dv_ring(j).near()
         weight_part(lax.rem(z + 1, 4), j)
         weight_part(lax.rem(z + 3, 4), j)
         return c
     with scope("late"):
-        lax.fori_loop(0, 4, late, 0)
+        lax.fori_loop(0, 5, late, 0)
+        for o in (1, 3):
+            send_head(o, False)
+        for o in (1, 3):
+            send_head(o, True)
 
     def distant(n, c):
         dv_ring(7 - n).far()
@@ -554,42 +537,33 @@
         return c
     with scope("distant"):
         lax.fori_loop(0, 8, distant, 0)
-
-    def out_rows(n, c):
-        for h in range(4):
-            gwp[n, :, :, h * 128:(h + 1) * 128] = gwt[h, :, rows(n, 128)].T.astype(BF).reshape(8, 16, 128)
-        return c
-    with scope("outrows"):
-        lax.fori_loop(0, 4, out_rows, 0)
-
-    def gw_part(d, src, to):
-        return remote(gwp.at[:, to], gwin.at[src], es.at[to], er.at[src], sp, d)
-    dp_peers(lambda d: gw_part(d, dp, d).start())
+    send_head(2, False)
+    send_head(2, True)
     dp_peers(lambda d: gl_part(d, dp, d).start())
-    gwin[dp] = gwp[:, dp]
     glin[dp] = glb[...]
-    with scope("wrownear"):
-        wrow.near()
-    with scope("dvwait"):
-        sp_peers(lambda s: dv_part(s, s, sp).wait_recv())
+    for h in range(4):
+        gwin[h, dp] = gwp[h, dp]
+        dvin[h, y] = dvg[h, 2 * z + lax.div(y, 2), rows(lax.rem(y, 2), 128), :]
     with scope("wrowfar"):
         wrow.far()
+    with scope("dvwait"):
+        all_of(dvin.at[pl.ds(0, 3)], dr)
+    for b in range(4):
+        for a in range(4):
+            dvrow[:, (4 * b + a) * 128:(4 * b + a + 1) * 128] = dvin[b, a]
     with scope("gwwait"):
-        dp_peers(lambda d: gw_part(d, d, dp).wait_recv())
-    acc = gwin[0].astype(F32)
-    for d in range(1, 8):
-        acc = acc + gwin[d].astype(F32)
-    gws[...] = acc.astype(BF)
-
-    def y_peers(body):
-        for d in (1, 3, 2):
-            body(lax.rem(y + d, 4))
+        all_of(gwin.at[:, pl.ds(0, 7)], er)
+    for h in range(4):
+        acc = gwin[h, 0].astype(F32)
+        for d in range(1, 8):
+            acc = acc + gwin[h, d].astype(F32)
+        gws[:, h] = acc.astype(BF)
 
     def fin_part(yy, src, to):
-        return remote(gws.at[to], gwf.at[src], fs.at[to], fr.at[src], z * 4 + yy, dp)
+        return remote(gws.at[to], gwf.at[src], fs.at[0], fr.at[0], z * 4 + yy, dp)
     y_peers(lambda t: fin_part(t, y, t).start())
     gwf[y] = gws[y]
-    dp_peers(lambda d: gl_part(d, d, dp).wait_recv())
+    all_of(glin.at[pl.ds(0, 7)], lr)
     tot = glin[0]
     for d in range(1, 8):
         tot = tot + glin[d]
@@ -608,35 +582,52 @@
     save_t = pltpu.make_async_copy(gtb, gt_h, save.at[2])
     save_t.start()
     with scope("finwait"):
-        y_peers(lambda t: fin_part(t, t, y).wait_recv())
+        all_of(gwf.at[pl.ds(0, 3)], fr)
     for a in range(4):
         for b in range(4):
-            gwo[:, (4 * b + a) * 128:(4 * b + a + 1) * 128] = gwf[a, :, b * 128:(b + 1) * 128].astype(F32)
+            gwo[:, (4 * b + a) * 128:(4 * b + a + 1) * 128] = gwf[a, b].astype(F32)
     save_w = pltpu.make_async_copy(gwo, gw_h, save.at[4])
     save_w.start()
     xring.drain()
     cring.drain()
-    wplane.drain()
+    wy.drain()
+    wz.drain()
     wrow.drain()
     qrow.drain()
-    lax.fori_loop(0, NB, lambda j, c: (dv_ring(j).drain(), c)[1], 0)
-    sp_peers(lambda s: head_rows(s, sp, s).wait_send())
-    sp_peers(lambda s: cot_part(s, sp, s).wait_send())
-    sp_peers(lambda s: dv_part(s, sp, s).wait_send())
-    z_peers(lambda t: columns(t, z, t).wait_send())
-    z_peers(lambda t: v_part(t, z, t).wait_send())
-    dp_peers(lambda d: gw_part(d, dp, d).wait_send())
-    dp_peers(lambda d: gl_part(d, dp, d).wait_send())
-    y_peers(lambda t: fin_part(t, y, t).wait_send())
+    all_of(dvg.at[pl.ds(0, 3)], gs)
+    all_of(wq.at[pl.ds(0, 15), 0], h1s)
+    all_of(cota.at[pl.ds(0, 1920)], cs)
+    all_of(dvin.at[pl.ds(0, 3)], ds_)
+    all_of(gwin.at[:, pl.ds(0, 7)], es)
+    all_of(xc.at[0, pl.ds(0, 3)], zs)
+    all_of(v4.at[pl.ds(0, 3)], vs)
+    all_of(glin.at[pl.ds(0, 7)], ls)
+    all_of(gwf.at[pl.ds(0, 3)], fs)
     with scope("savewait"):
         for a in (save_k, save_q, save_t, save_l, save_w):
             a.wait()
+
+
+def hand_out(*refs):
+    came, outs, held, (got, put) = refs[:5], refs[5:10], refs[10:15], refs[15:]
+    loads = [pltpu.make_async_copy(came[n], held[n], got.at[n]) for n in range(5)]
+    saves = [pltpu.make_async_copy(held[n], outs[n], put.at[n]) for n in range(4)]
+    for a in loads:
+        a.start()
+    for n in range(4):
+        loads[n].wait()
+        saves[n].start()
+    loads[4].wait()
+    outs[4][0] = held[4][0, 0]
+    for a in saves:
+        a.wait()
 
 
 def body(tokens, cotangent, value_weight, query_heads, key_heads, lambdas):
     L = query_heads.shape[1]
     smem = pl.BlockSpec(memory_space=pltpu.SMEM)
     anywhere = pl.BlockSpec(memory_space=pl.ANY)
+    hbm = pl.BlockSpec(memory_space=pltpu.HBM)
     tiles = (NB * (NB + 1) // 2, B, B)
     dma = lambda *n: pltpu.SemaphoreType.DMA(n)
     gq, gk, gt, gw, gl = pl.pallas_call(
@@ -649,15 +640,20 @@
             V((NB, B, 128), BF), V((NB, B, 128), BF), V((NB, 128, B), BF), V((NB, 128, B), BF), V((NB, B, 128), BF), V((4, 2, B, 128), BF),
             V((NB, B, B), F32), V((NB, B, B), F32), V(tiles, BF), V(tiles, BF), V(tiles, BF),
             V((NB, 128, B), BF), V((NB, B, 128), BF), V((NB, 8, B), F32), V((NB, 128, B), F32), V((NB, 128, B), F32), V((NB, 128, B), F32),
-            V((4, NB, B, 128), BF), V((128, 2048), BF), V((4, 128, 512), F32), V((4, 8, 16, 512), BF), V((8, 4, 16, 512), BF),
-            V((4, 16, 512), BF), V((4, 16, 512), BF), V((L, 128), BF), V((L, 128), BF), V((128, 2048), BF), V((16, 2048), F32),
+            V((4, NB, B, 128), BF), V((4, 4, 128, 128), BF), V((128, 2048), BF), V((4, 128, 512), F32), V((4, 8, 4, 16, 128), BF), V((4, 8, 4, 16, 128), BF),
+            V((4, 4, 16, 128), BF), V((4, 4, 16, 128), BF), V((L, 128), BF), V((L, 128), BF), V((128, 2048), BF), V((16, 2048), F32),
             V((8, 128), F32), V((8, 8, 128), F32),
-            dma(5), dma(4, 4), dma(5), dma(4), dma(4), dma(4), dma(4), dma(4), dma(4), dma(2, 20), dma(2, 20), dma(8), dma(8), dma(8), dma(8),
-            dma(16), dma(16), dma(16), dma(16), dma(4), dma(4), dma(8, 4), dma(8, 4), dma(16), dma(16),
-            dma(8), dma(8), dma(8), dma(8), dma(4), dma(4)],
+            dma(5), dma(1), dma(5), dma(6), dma(6), dma(4), dma(4), dma(1), dma(1), dma(2, 4), dma(2, 4), dma(8), dma(8), dma(8), dma(8), dma(1), dma(1), dma(1), dma(1), dma(1), dma(4), dma(1), dma(8, 4), dma(1), dma(1), dma(1), dma(1), dma(1), dma(1), dma(1), dma(1)],
         compiler_params=pltpu.CompilerParams(vmem_limit_bytes=60 * 1024 * 1024, collective_id=0, has_side_effects=True),
         name="whole")(lambdas, tokens[0], cotangent[0], value_weight, query_heads.reshape(L, 128), key_heads.reshape(L, 128))
-    return gq.reshape(query_heads.shape), gk.reshape(key_heads.shape), gt[None], gw, gl[0, 0:1]
+    gq, gk, gt, gw, gl = pl.pallas_call(
+        hand_out,
+        out_shape=(S((L, 128), BF), S((L, 128), BF), S((128, 2048), BF), S((16, 2048), F32), S((1,), F32)),
+        in_specs=[hbm] * 5, out_specs=[hbm] * 4 + [smem],
+        scratch_shapes=[V((L, 128), BF), V((L, 128), BF), V((128, 2048), BF), V((16, 2048), F32), pltpu.SMEM((8, 128), F32), dma(5), dma(4)],
+        compiler_params=pltpu.CompilerParams(vmem_limit_bytes=60 * 1024 * 1024),
+        name="hand_out")(gq, gk, gt, gw, gl)
+    return gq.reshape(query_heads.shape), gk.reshape(key_heads.shape), gt[None], gw, gl
 
 
 def solution(mesh):

time: 118 us -> 89.9 us (0.76)
  Pallas kernels: 110 us -> 87.9 us
  local copies, waits for them, and re-layouts: 6.03 us -> 0 us
    pallas_call x1, Pallas kernels: 110 us -> 85.1 us  [body(): pl.pallas_call(kernel, out_shape=(S((L, 128), BF), S((L, 128), BF), S((12...]
    unnamed x10 -> x0, local copies, waits for them, and re-layouts: 4.84 us -> none
    pallas_call x0 -> x1, Pallas kernels: none -> 2.81 us  [body(): pl.pallas_call(hand_out, out_shape=(S((L, 128), BF), S((L, 128), BF), S((...]
    slice x1 -> x0, local copies, waits for them, and re-layouts: 1.19 us -> none  [body(): gl[0, 0:1]]
where the time goes in v3:
time: 89.9 us; the launch traced here: 89.2 us
  Pallas kernels  87.9 us (98%)
  between operations  1.29 us (1%)
    pallas_call x1, Pallas kernels, body(): pl.pallas_call(kernel, out_shape=(S((L, 128), BF), S((L, 128), BF), S((12...  85.1 us
    pallas_call x1, Pallas kernels, body(): pl.pallas_call(hand_out, out_shape=(S((L, 128), BF), S((L, 128), BF), S((...  2.81 us

profile of v3, /device:TPU:1, one launch (start us, length us, event | category | flops | bytes accessed | tf_op | source)
XLA Modules:
  0.0 89.2 jit_solution(2796575365508374484)
XLA Ops:
  1.3 85.1 %whole.1 = (bf16[2048,128]{1,0:T(8,128)(2,1)}, bf16[2048,128]{1,0:T(8,128)(2,1)}, bf16[128,2048]{1,0:T(8,128)(2,1)}, f32[16,2048]{1,0:T(8,128)}, f32[8,128]{1,0:T(8,128)}) custom-call(f32[1]{0:T(128)S(6)} %copy.11.lam_ref, bf16[128,2048]{1,0:T(8,128)(2,1)} %bitcast.7, bf16[128,2048]{1,0:T(8,128)(2,1)} %bitcast.8, bf16[16,2048]{1,0:T(8,128)(2,1)} %w_h.1, ...), custom_call_target="tpu_custom_call" | custom-call | tf_op jit(solution)/shard_map/whole/pallas_call | solution.py:633
  86.4 2.8 %hand_out.1 = (bf16[2048,128]{1,0:T(8,128)(2,1)}, bf16[2048,128]{1,0:T(8,128)(2,1)}, bf16[128,2048]{1,0:T(8,128)(2,1)}, f32[16,2048]{1,0:T(8,128)}, f32[1]{0:T(128)}) custom-call(bf16[2048,128]{1,0:T(8,128)(2,1)} %get-tuple-element.15.refs_0_, bf16[2048,128]{1,0:T(8,128)(2,1)} %get-tuple-element.16.refs_1_, bf16[128,2048]{1,0:T(8,128)(2,1)} %get-tuple-element.17.refs_2_, ...), custom_call_target="tpu_custom_call" | custom-call | tf_op jit(solution)/shard_map/hand_out/pallas_call | solution.py:649

commit v4 on v3

--- a/solution.py
+++ b/solution.py
@@ -133,118 +133,49 @@
 
 
 class Ring:
-    def __init__(self, at, ss, rs, sp, dp, axis):
-        self.at, self.ss, self.rs, self.sp, self.dp, self.axis = at, ss, rs, sp, dp, axis
+    def __init__(self, at, ss, rs, me, to):
+        self.at, self.ss, self.rs, self.me, self.to = at, ss, rs, me, to
 
     def index(self, o):
-        return lax.rem((lax.rem(self.sp, 4) if self.axis == 0 else lax.div(self.sp, 4)) + (o + 4), 4)
-
-    def copy(self, slot, o, part, delta):
-        i = self.index(delta)
-        to = lax.div(self.sp, 4) * 4 + i if self.axis == 0 else i * 4 + lax.rem(self.sp, 4)
+        return lax.rem(self.me + (o + 4), 4)
+
+    def copy(self, o, part, delta, sem):
+        s, d = self.to(self.index(delta))
         ref = self.at(self.index(o), part)
         return pltpu.make_async_remote_copy(
-            src_ref=ref, dst_ref=ref, send_sem=self.ss(slot), recv_sem=self.rs(slot),
-            device_id={"sp": to, "dp": self.dp}, device_id_type=MESH)
+            src_ref=ref, dst_ref=ref, send_sem=self.ss, recv_sem=self.rs(sem),
+            device_id={"sp": s, "dp": d}, device_id_type=MESH)
 
     def start(self):
-        self.copy(0, 0, None, 1).start()
-        self.copy(1, 0, None, -1).start()
+        self.copy(0, 0, 1, 0).start()
+        self.copy(0, 1, -1, 1).start()
+        self.copy(0, 1, 1, 2).start()
+        self.copy(0, 0, -1, 2).start()
 
     def near(self):
-        self.copy(0, -1, None, 1).wait_recv()
-        self.copy(2, -1, 0, 1).start()
-        self.copy(1, 1, None, -1).wait_recv()
-        self.copy(3, 1, 1, -1).start()
+        self.copy(-1, 0, 1, 0).wait_recv()
+        self.copy(-1, 0, 1, 3).start()
+        self.copy(1, 1, -1, 1).wait_recv()
+        self.copy(1, 1, -1, 3).start()
+
+    def both(self, o, sem):
+        ref = self.at(self.index(o), None)
+        pltpu.make_async_copy(ref, ref, self.rs(sem)).wait()
+
+    def full(self):
+        self.both(1, 2)
 
     def far(self):
-        self.copy(2, 2, 0, 1).wait_recv()
-        self.copy(3, 2, 1, 1).wait_recv()
-
-    def drain(self):
-        for slot in range(4):
-            self.copy(slot, 0, None if slot < 2 else slot - 2, 1).wait_send()
-
-
-class SplitRing(Ring):
-    def start(self, n):
-        self.copy(2 * n, 0, n, 1).start()
-        self.copy(2 * n + 1, 0, n, -1).start()
-
-    def near(self, n):
-        if n == 0:
-            self.copy(0, -1, 0, 1).wait_recv()
-            self.copy(4, -1, 0, 1).start()
-            self.copy(1, 1, 0, -1).wait_recv()
-        else:
-            self.copy(3, 1, 1, -1).wait_recv()
-            self.copy(5, 1, 1, -1).start()
-            self.copy(2, -1, 1, 1).wait_recv()
-
-    def far(self):
-        self.copy(4, 2, 0, 1).wait_recv()
-        self.copy(5, 2, 1, -1).wait_recv()
-
-    def drain(self):
-        for slot, n in enumerate((0, 0, 1, 1, 0, 1)):
-            self.copy(slot, 0, n, 1).wait_send()
-
-
-class Row:
-    def __init__(self, w, ss, rs, sp, dp):
-        self.w, self.ss, self.rs, self.sp, self.dp = w, ss, rs, sp, dp
-        self.x, self.c = lax.div(dp, 2), lax.rem(dp, 2)
-
-    def own(self, o):
-        return 2 * lax.rem(self.x + (o + 4), 4) + self.c
-
-    def copy(self, slot, o, to, half=None):
-        part = pl.ds(0, 16) if half is None else pl.ds(8 * half, 8)
-        return pltpu.make_async_remote_copy(
-            src_ref=self.w.at[part, self.own(o)], dst_ref=self.w.at[part, self.own(o)],
-            send_sem=self.ss.at[slot], recv_sem=self.rs.at[slot],
-            device_id={"sp": self.sp, "dp": to}, device_id_type=MESH)
-
-    def other(self, slot, o):
-        return self.copy(slot, o, self.dp + 1 - 2 * self.c)
-
-    def start(self):
-        self.copy(0, 0, self.own(1)).start()
-        self.copy(1, 0, self.own(-1)).start()
-        self.other(4, 0).start()
-
-    def near(self):
-        self.copy(0, -1, self.own(1)).wait_recv()
-        self.copy(2, -1, self.own(1), 0).start()
-        self.other(5, -1).start()
-        self.copy(1, 1, self.own(-1)).wait_recv()
-        self.copy(3, 1, self.own(-1), 1).start()
-        self.other(6, 1).start()
-
-    def far(self):
-        self.copy(2, 2, self.own(1), 0).wait_recv()
-        self.copy(3, 2, self.own(1), 1).wait_recv()
-        self.other(7, 2).start()
-
-    def arrived(self):
-        for slot in (4, 5, 6, 7):
-            self.other(slot, 0).wait_recv()
-
-    def drain(self):
-        for slot in (0, 1, 4, 5, 6, 7):
-            self.copy(slot, 0, self.own(1)).wait_send()
-        for slot in (2, 3):
-            self.copy(slot, 0, self.own(1), 0).wait_send()
-
-
-def kernel(lam_ref, tok_h, cot_h, w_h, q_h, k_h, gq_h, gk_h, gt_h, gw_h, gl_h,
+        self.both(2, 3)
+
+
+def kernel(lam_h, tok_h, cot_h, w_h, q_h, k_h, gq_h, gk_h, gt_h, gw_h, gl_h,
            xr, xc, w, wo, wq, cota, q_ref, k_ref, qz1, qz2, kt, vt, vn, v4, s1, s2, p1, p2, aa, dot, do, delta, dqt, ot, o2t,
-           dvg, dvin, dvrow, gwt, gwp, gwin, gws, gwf, gqb, gkb, gtb, gwo, glb, glin,
-           load, wload, save, xs, xr_, ys, yr, zs, zr, ws, wr, rs_, rr, qs, qr, h1s, h1r, cs, cr, vs, vr, gs, gr, ds_, dr,
-           es, er, ls, lr, fs, fr):
+           dvg, dvin, dvrow, gta, gwt, gwp, gwin, gws, gwf, gqb, gkb, gtb, gwo, glb, glin,
+           lam_ref, load, wload, save, xs, xr_, ys, yr, zs, zr, ws, wr, rs_, rr, qs, qr, h1s, h1r, cs, cr, vs, vr, gs, gr, ds_, dr,
+           es, er, ls, lr, fs, fr, wds, wdr, qds, qdr):
     sp, dp = lax.axis_index("sp"), lax.axis_index("dp")
     y, z = lax.rem(sp, 4), lax.div(sp, 4)
-    lam = lam_ref[0]
     scope = jax.named_scope
 
     def sp_peers(body):
@@ -270,7 +201,7 @@
     sp_peers(lambda s: pl.semaphore_signal(barrier, inc=1, device_id={"sp": s, "dp": dp}, device_id_type=MESH))
     dp_peers(lambda d: pl.semaphore_signal(barrier, inc=1, device_id={"sp": sp, "dp": d}, device_id_type=MESH))
     loads = [pltpu.make_async_copy(a, b, load.at[n]) for n, (a, b) in enumerate((
-        (w_h, w.at[sp, dp]), (tok_h, xr.at[y]), (q_h, q_ref), (k_h, k_ref), (cot_h.at[:, lanes(sp)], cota.at[rows(sp, 128)])))]
+        (w_h, w.at[sp, dp]), (tok_h, xr.at[y]), (q_h, q_ref), (k_h, k_ref), (cot_h.at[:, lanes(sp)], cota.at[rows(sp, 128)]), (lam_h, lam_ref)))]
     for a in loads:
         a.start()
     parts = [pltpu.make_async_copy(w_h.at[:, pl.ds((4 * b + a) * 128, 128)], wo.at[a, :, pl.ds(b * 128, 128)], wload.at[0])
@@ -278,18 +209,27 @@
     for a in parts:
         a.start()
 
-    def half_rows(ref):
-        return lambda i, part: ref.at[i] if part is None else ref.at[i, pl.ds(64 * part, 64)]
+    x_, core = lax.div(dp, 2), lax.rem(dp, 2)
+    along_y = lambda i: (z * 4 + i, dp)
+    along_z = lambda i: (i * 4 + y, dp)
+    along_x = lambda i: (sp, 2 * i + core)
+
+    def split(ref, view, n):
+        return lambda i, part: view(i, pl.ds(0, n) if part is None else pl.ds(n // 2 * part, n // 2))
 
     wy = Ring(lambda i, part: w.at[z * 4 + i, dp] if part is None else w.at[z * 4 + i, dp, :, pl.ds(1024 * part, 1024)],
-              lambda n: ws.at[0, n], lambda n: wr.at[0, n], sp, dp, 0)
+              ws.at[0], lambda n: wr.at[0, n], y, along_y)
     wz = Ring(lambda i, part: w.at[pl.ds(4 * i, 4), dp] if part is None else w.at[pl.ds(4 * i + 2 * part, 2), dp],
-              lambda n: ws.at[1, n], lambda n: wr.at[1, n], sp, dp, 1)
-    xring = SplitRing(half_rows(xr), lambda n: xs.at[n], lambda n: xr_.at[n], sp, dp, 0)
-    cring = Ring(lambda i, part: xc.at[i] if part is None else xc.at[i, pl.ds(2 * part, 2)],
-                 lambda n: ys.at[n], lambda n: yr.at[n], sp, dp, 0)
-    wrow = Row(w, rs_, rr, sp, dp)
-    qrow = Row(wq, qs, qr, sp, dp)
+              ws.at[1], lambda n: wr.at[1, n], z, along_z)
+    xring = Ring(split(xr, lambda i, d: xr.at[i, d], 128), xs.at[0], lambda n: xr_.at[n], y, along_y)
+    cring = Ring(split(xc, lambda i, d: xc.at[i, d], 4), ys.at[0], lambda n: yr.at[n], y, along_y)
+    wrow = Ring(split(w, lambda i, d: w.at[d, 2 * i + core], 16), rs_.at[0], lambda n: rr.at[n], x_, along_x)
+    qrow = Ring(split(wq, lambda i, d: wq.at[d, 2 * i + core], 16), qs.at[0], lambda n: qr.at[n], x_, along_x)
+
+    def other(ref, ring, o, ss, rs):
+        d = 2 * ring.index(o) + core
+        return remote(ref.at[:, d], ref.at[:, d], ss.at[0], rs.at[0], sp, dp + 1 - 2 * core)
+
     for a in loads[:2]:
         a.wait()
     all_of(wo, wload)
@@ -308,15 +248,15 @@
         for d in (1, 3, 2):
             body(lax.rem(z + d, 4))
 
+    wy.start()
     sp_peers(lambda s: head_rows(s, sp, s).start())
-    wy.start()
-    xring.start(0)
     z_peers(lambda t: columns(t, z, t).start())
     def cot_part(s, src, to):
         return remote(cot_h.at[:, lanes(to)], cota.at[rows(src, 128)], cs.at[0], cr.at[0], s, dp)
 
-    for n in (2, 3):
+    for n in (2, 3, 5):
         loads[n].wait()
+    lam = lam_ref[0]
 
     def prep(i, c):
         prepare(i, q_ref, k_ref, qz1, qz2, kt)
@@ -332,39 +272,50 @@
 
     with scope("soft03"):
         soft(0, 3)
+    with scope("wynear"):
+        wy.near()
+    xring.start()
     with scope("heads"):
         all_of(wq.at[pl.ds(0, 15), 0], h1r)
     qrow.start()
-    with scope("wynear"):
-        wy.near()
-    xring.start(1)
-    with scope("soft35"):
-        soft(3, 5)
-    with scope("xnear0"):
-        xring.near(0)
-    with scope("soft56"):
-        soft(5, 6)
+    other(wq, qrow, 0, qds, qdr).start()
+    with scope("soft34"):
+        soft(3, 4)
     with scope("wyfar"):
+        wy.full()
         wy.far()
     wz.start()
+    with scope("soft46"):
+        soft(4, 6)
+    with scope("xnear0"):
+        xring.near()
     with scope("soft67"):
         soft(6, 7)
     with scope("qnear"):
         qrow.near()
-    with scope("xnear1"):
-        xring.near(1)
+        qrow.full()
+        for o in (-1, 1):
+            other(wq, qrow, o, qds, qdr).start()
+    with scope("wznear"):
+        wz.near()
+    with scope("xfull"):
+        xring.full()
     sp_peers(lambda s: cot_part(s, sp, s).start())
     with scope("columns"):
         all_of(xc.at[0, pl.ds(0, 3)], zr)
     cring.start()
     with scope("soft78"):
         soft(7, 8)
-    with scope("wznear"):
-        wz.near()
+    with scope("wzfar"):
+        wz.full()
+        wz.far()
+    wrow.start()
+    other(w, wrow, 0, wds, wdr).start()
     with scope("qfar"):
         qrow.far()
+        other(wq, qrow, 2, qds, qdr).start()
     with scope("qall"):
-        qrow.arrived()
+        all_of(wq.at[:, pl.ds(0, 4)], qdr)
     with scope("xfar"):
         xring.far()
 
@@ -382,9 +333,6 @@
                 def _():
                     v_part(t, z, t).start()
         vn[pl.ds(2 * z, 2)] = v4[z]
-    with scope("wzfar"):
-        wz.far()
-    wrow.start()
 
     def mixed(r):
         def one(e, c):
@@ -444,7 +392,7 @@
 
     def dv_part(yy, src, to, h):
         part = rows(lax.rem(to, 2), 128)
-        return remote(dvg.at[h, 2 * z + lax.div(to, 2), part], dvin.at[h, src], ds_.at[0], dr.at[0], z * 4 + yy, dp)
+        return remote(dvg.at[h, 2 * z + lax.div(to, 2), part], dvin.at[h, src], ds_.at[0], dr.at[h], z * 4 + yy, dp)
 
     def y_peers(body):
         for d in (1, 3, 2):
@@ -464,27 +412,42 @@
 
     def dv_ring(j):
         return Ring(lambda i, part: dvg.at[i, j] if part is None else dvg.at[i, j, pl.ds(128 * part, 128)],
-                    lambda n: gs.at[0], lambda n: gr.at[j, n], sp, dp, 1)
+                    gs.at[0], lambda n: gr.at[j, n], z, along_z)
 
     def main(n, c):
         j = NB - 1 - n
         dv, dk1, dk2 = keys_block(j, vn, qz1, qz2, kt, p1, p2, aa, dot, do, delta, dqt)
         dvg[z, j] = dv.astype(BF)
+        dv_ring(j).start()
         gkb[rows(j), :] = ((dk1 + dk2) * ks).astype(BF)
-        dv_ring(j).start()
-
-        @pl.when(n >= 5)
+
+        @pl.when(n == 2)
         def _():
-            dv_ring(j + 5).near()
+            wrow.near()
+
+        @pl.when(n == 4)
+        def _():
+            cring.near()
+            dv_ring(7).near()
 
         @pl.when(n == 5)
         def _():
-            cring.near()
+            dv_ring(6).near()
+
+        @pl.when(n == 6)
+        def _():
+            dv_ring(5).near()
+
+        @pl.when(n == 7)
+        def _():
+            dv_ring(4).near()
+            wrow.full()
+            for o in (-1, 1):
+                other(w, wrow, o, wds, wdr).start()
         return c
     with scope("main"):
         lax.fori_loop(0, NB, main, 0)
-    with scope("wrownear"):
-        wrow.near()
+    send_head(0, False)
     save_k = pltpu.make_async_copy(gkb, gk_h, save.at[0])
     save_k.start()
 
@@ -509,48 +472,73 @@
             return c
         lax.fori_loop(lo, hi, one, 0)
 
+    with scope("near3"):
+        dv_ring(3).near()
     with scope("cfar"):
+        cring.full()
         cring.far()
-    send_head(0, False)
     with scope("pieces0"):
         pieces(0, 8, (0,))
         send_head(0, True)
+    with scope("near2"):
+        dv_ring(2).near()
+    with scope("near1"):
+        dv_ring(1).near()
+
+    def neighbours(lo, hi):
+        def one(n, c):
+            j = hi - 1 - n
+            dv_ring(j).full()
+            weight_part(lax.rem(z + 1, 4), j)
+            weight_part(lax.rem(z + 3, 4), j)
+            return c
+        lax.fori_loop(0, hi - lo, one, 0)
     with scope("pieces13"):
-        pieces(5, 8, (1, 3))
-
-    def late(n, c):
-        j = 4 - n
-        dv_ring(j).near()
-        weight_part(lax.rem(z + 1, 4), j)
-        weight_part(lax.rem(z + 3, 4), j)
-        return c
-    with scope("late"):
-        lax.fori_loop(0, 5, late, 0)
-        for o in (1, 3):
-            send_head(o, False)
-        for o in (1, 3):
-            send_head(o, True)
-
-    def distant(n, c):
-        dv_ring(7 - n).far()
-        weight_part(lax.rem(z + 2, 4), 7 - n)
-        return c
+        neighbours(2, 8)
+    with scope("near0"):
+        dv_ring(0).near()
+    with scope("pieces01"):
+        neighbours(0, 2)
+    for o in (1, 3):
+        send_head(o, False)
+    for o in (1, 3):
+        send_head(o, True)
+
+    def gather(o):
+        h = lax.rem(z + o, 4)
+        dvin[h, y] = dvg[h, 2 * z + lax.div(y, 2), rows(lax.rem(y, 2), 128), :]
+        pltpu.make_async_copy(dvin.at[h, pl.ds(0, 3)], dvin.at[h, pl.ds(0, 3)], dr.at[h]).wait()
+        for a in range(4):
+            dvrow[h, :, a * 128:(a + 1) * 128] = dvin[h, a]
+
+    def times_rows(n, o):
+        h = lax.rem(z + o, 4)
+        return nt(dvrow[h], w[pl.ds(2 * n, 2), :, :, lanes(h, 512)].reshape(B, 512))
+
+    with scope("wrowfar"):
+        wrow.far()
+        other(w, wrow, 2, wds, wdr).start()
+    with scope("far"):
+        lax.fori_loop(0, NB, lambda n, c: (dv_ring(7 - n).far(), c)[1], 0)
+    send_head(2, False)
     with scope("distant"):
-        lax.fori_loop(0, 8, distant, 0)
-    send_head(2, False)
+        pieces(0, 8, (2,))
     send_head(2, True)
     dp_peers(lambda d: gl_part(d, dp, d).start())
     glin[dp] = glb[...]
     for h in range(4):
         gwin[h, dp] = gwp[h, dp]
-        dvin[h, y] = dvg[h, 2 * z + lax.div(y, 2), rows(lax.rem(y, 2), 128), :]
-    with scope("wrowfar"):
-        wrow.far()
-    with scope("dvwait"):
-        all_of(dvin.at[pl.ds(0, 3)], dr)
-    for b in range(4):
-        for a in range(4):
-            dvrow[:, (4 * b + a) * 128:(4 * b + a + 1) * 128] = dvin[b, a]
+    with scope("gather"):
+        for o in (0, 1, 3):
+            gather(o)
+    with scope("wrowall"):
+        all_of(w.at[:, pl.ds(0, 4)], wdr)
+
+    def most(n, c):
+        gta[:, rows(n)] = times_rows(n, 0) + times_rows(n, 1) + times_rows(n, 3)
+        return c
+    with scope("tgrada"):
+        lax.fori_loop(0, NB, most, 0)
     with scope("gwwait"):
         all_of(gwin.at[:, pl.ds(0, 7)], er)
     for h in range(4):
@@ -570,14 +558,13 @@
     delta[0] = jnp.concatenate([tot, tot], axis=1)
     save_l = pltpu.make_async_copy(delta.at[0, :, pl.ds(0, 128)], gl_h, save.at[3])
     save_l.start()
-    with scope("wrowall"):
-        wrow.arrived()
+    with scope("dvwait"):
+        gather(2)
 
     def tokens_grad(n, c):
-        g = nt(dvrow[...], w[pl.ds(2 * n, 2)].reshape(B, 2048))
-        gtb[:, rows(n)] = g.astype(BF)
+        gtb[:, rows(n)] = (gta[:, rows(n)] + times_rows(n, 2)).astype(BF)
         return c
-    with scope("tgrad"):
+    with scope("tgradb"):
         lax.fori_loop(0, NB, tokens_grad, 0)
     save_t = pltpu.make_async_copy(gtb, gt_h, save.at[2])
     save_t.start()
@@ -588,12 +575,14 @@
             gwo[:, (4 * b + a) * 128:(4 * b + a + 1) * 128] = gwf[a, b].astype(F32)
     save_w = pltpu.make_async_copy(gwo, gw_h, save.at[4])
     save_w.start()
-    xring.drain()
-    cring.drain()
-    wy.drain()
-    wz.drain()
-    wrow.drain()
-    qrow.drain()
+    all_of(xr.at[pl.ds(0, 3)], xs)
+    all_of(xc.at[pl.ds(0, 3)], ys)
+    all_of(w.at[pl.ds(0, 3), 0], ws)
+    pltpu.make_async_copy(w.at[pl.ds(0, 12), 0], w.at[pl.ds(0, 12), 0], ws.at[1]).wait()
+    all_of(w.at[:, pl.ds(0, 3)], rs_)
+    all_of(wq.at[:, pl.ds(0, 3)], qs)
+    all_of(w.at[:, pl.ds(0, 4)], wds)
+    all_of(wq.at[:, pl.ds(0, 4)], qds)
     all_of(dvg.at[pl.ds(0, 3)], gs)
     all_of(wq.at[pl.ds(0, 15), 0], h1s)
     all_of(cota.at[pl.ds(0, 1920)], cs)
@@ -633,17 +622,17 @@
     gq, gk, gt, gw, gl = pl.pallas_call(
         kernel,
         out_shape=(S((L, 128), BF), S((L, 128), BF), S((128, 2048), BF), S((16, 2048), F32), S((8, 128), F32)),
-        in_specs=[smem] + [anywhere] * 5, out_specs=[anywhere] * 5,
+        in_specs=[anywhere] * 6, out_specs=[anywhere] * 5,
         scratch_shapes=[
             V((4, 128, 2048), BF), V((4, 4, 128, 512), BF), V((16, 8, 16, 2048), BF), V((4, 16, 512), BF), V((16, 8, 16, 512), BF),
             V((L, 128), BF), V((L, 128), BF), V((L, 128), BF),
             V((NB, B, 128), BF), V((NB, B, 128), BF), V((NB, 128, B), BF), V((NB, 128, B), BF), V((NB, B, 128), BF), V((4, 2, B, 128), BF),
             V((NB, B, B), F32), V((NB, B, B), F32), V(tiles, BF), V(tiles, BF), V(tiles, BF),
             V((NB, 128, B), BF), V((NB, B, 128), BF), V((NB, 8, B), F32), V((NB, 128, B), F32), V((NB, 128, B), F32), V((NB, 128, B), F32),
-            V((4, NB, B, 128), BF), V((4, 4, 128, 128), BF), V((128, 2048), BF), V((4, 128, 512), F32), V((4, 8, 4, 16, 128), BF), V((4, 8, 4, 16, 128), BF),
+            V((4, NB, B, 128), BF), V((4, 4, 128, 128), BF), V((4, 128, 512), BF), V((128, 2048), F32), V((4, 128, 512), F32), V((4, 8, 4, 16, 128), BF), V((4, 8, 4, 16, 128), BF),
             V((4, 4, 16, 128), BF), V((4, 4, 16, 128), BF), V((L, 128), BF), V((L, 128), BF), V((128, 2048), BF), V((16, 2048), F32),
-            V((8, 128), F32), V((8, 8, 128), F32),
-            dma(5), dma(1), dma(5), dma(6), dma(6), dma(4), dma(4), dma(1), dma(1), dma(2, 4), dma(2, 4), dma(8), dma(8), dma(8), dma(8), dma(1), dma(1), dma(1), dma(1), dma(1), dma(4), dma(1), dma(8, 4), dma(1), dma(1), dma(1), dma(1), dma(1), dma(1), dma(1), dma(1)],
+            V((8, 128), F32), V((8, 8, 128), F32), pltpu.SMEM((1,), F32),
+            dma(6), dma(1), dma(5), dma(1), dma(4), dma(1), dma(4), dma(1), dma(1), dma(2), dma(2, 4), dma(1), dma(4), dma(1), dma(4), dma(1), dma(1), dma(1), dma(1), dma(1), dma(4), dma(1), dma(8, 4), dma(1), dma(4), dma(1), dma(1), dma(1), dma(1), dma(1), dma(1), dma(1), dma(1), dma(1), dma(1)],
         compiler_params=pltpu.CompilerParams(vmem_limit_bytes=60 * 1024 * 1024, collective_id=0, has_side_effects=True),
         name="whole")(lambdas, tokens[0], cotangent[0], value_weight, query_heads.reshape(L, 128), key_heads.reshape(L, 128))
     gq, gk, gt, gw, gl = pl.pallas_call(

time: 89.9 us -> 84.4 us (0.939)
  Pallas kernels: 87.9 us -> 82.9 us
    pallas_call x1, Pallas kernels: 85.1 us -> 80.1 us  [body(): pl.pallas_call(kernel, out_shape=(S((L, 128), BF), S((L, 128), BF), S((12...]
where the time goes in v4:
time: 84.4 us; the launch traced here: 84.2 us
  Pallas kernels  82.9 us (98%)
  between operations  1.29 us (2%)
    pallas_call x1, Pallas kernels, body(): pl.pallas_call(kernel, out_shape=(S((L, 128), BF), S((L, 128), BF), S((12...  80.1 us
    pallas_call x1, Pallas kernels, body(): pl.pallas_call(hand_out, out_shape=(S((L, 128), BF), S((L, 128), BF), S((...  2.81 us

profile of v4, /device:TPU:1, one launch (start us, length us, event | category | flops | bytes accessed | tf_op | source)
XLA Modules:
  0.0 84.2 jit_solution(2921085226853742935)
XLA Ops:
  1.3 80.1 %whole.1 = (bf16[2048,128]{1,0:T(8,128)(2,1)}, bf16[2048,128]{1,0:T(8,128)(2,1)}, bf16[128,2048]{1,0:T(8,128)(2,1)}, f32[16,2048]{1,0:T(8,128)}, f32[8,128]{1,0:T(8,128)}) custom-call(f32[1]{0:T(128)S(6)} %copy.11.lam_h, bf16[128,2048]{1,0:T(8,128)(2,1)} %bitcast.7, bf16[128,2048]{1,0:T(8,128)(2,1)} %bitcast.8, bf16[16,2048]{1,0:T(8,128)(2,1)} %w_h.1, ...), custom_call_target="tpu_custom_call" | custom-call | tf_op jit(solution)/shard_map/whole/pallas_call | solution.py:622
  81.4 2.8 %hand_out.1 = (bf16[2048,128]{1,0:T(8,128)(2,1)}, bf16[2048,128]{1,0:T(8,128)(2,1)}, bf16[128,2048]{1,0:T(8,128)(2,1)}, f32[16,2048]{1,0:T(8,128)}, f32[1]{0:T(128)}) custom-call(bf16[2048,128]{1,0:T(8,128)(2,1)} %get-tuple-element.15.refs_0_, bf16[2048,128]{1,0:T(8,128)(2,1)} %get-tuple-element.16.refs_1_, bf16[128,2048]{1,0:T(8,128)(2,1)} %get-tuple-element.17.refs_2_, ...), custom_call_target="tpu_custom_call" | custom-call | tf_op jit(solution)/shard_map/hand_out/pallas_call | solution.py:638

commit v5 on v4

--- a/solution.py
+++ b/solution.py
@@ -171,9 +171,9 @@
 
 def kernel(lam_h, tok_h, cot_h, w_h, q_h, k_h, gq_h, gk_h, gt_h, gw_h, gl_h,
            xr, xc, w, wo, wq, cota, q_ref, k_ref, qz1, qz2, kt, vt, vn, v4, s1, s2, p1, p2, aa, dot, do, delta, dqt, ot, o2t,
-           dvg, dvin, dvrow, gta, gwt, gwp, gwin, gws, gwf, gqb, gkb, gtb, gwo, glb, glin,
+           dvg, dvin, dvrow, gta, gwp, gwin, gws, gwf, gqb, gkb, gtb, gwo, glb, glin,
            lam_ref, load, wload, save, xs, xr_, ys, yr, zs, zr, ws, wr, rs_, rr, qs, qr, h1s, h1r, cs, cr, vs, vr, gs, gr, ds_, dr,
-           es, er, ls, lr, fs, fr, wds, wdr, qds, qdr):
+           es, er, ls, lr, fs, fr, wds, wdr, qds, qdr, gf):
     sp, dp = lax.axis_index("sp"), lax.axis_index("dp")
     y, z = lax.rem(sp, 4), lax.div(sp, 4)
     scope = jax.named_scope
@@ -298,12 +298,9 @@
             other(wq, qrow, o, qds, qdr).start()
     with scope("wznear"):
         wz.near()
+    sp_peers(lambda s: cot_part(s, sp, s).start())
     with scope("xfull"):
         xring.full()
-    sp_peers(lambda s: cot_part(s, sp, s).start())
-    with scope("columns"):
-        all_of(xc.at[0, pl.ds(0, 3)], zr)
-    cring.start()
     with scope("soft78"):
         soft(7, 8)
     with scope("wzfar"):
@@ -316,23 +313,28 @@
         other(wq, qrow, 2, qds, qdr).start()
     with scope("qall"):
         all_of(wq.at[:, pl.ds(0, 4)], qdr)
+    def v_part(zz, src, to, b):
+        return remote(v4.at[to, b], vn.at[2 * src + lax.div(b, 2), rows(lax.rem(b, 2), 128)], vs.at[0], vr.at[src], zz * 4 + y, dp)
+
+    def values(b):
+        v = nn(xr[b], wq[...].reshape(2048, 512)).astype(BF)
+        for t in range(4):
+            v4[t, b] = v[:, t * 128:(t + 1) * 128]
+
+            @pl.when(t != z)
+            def _():
+                v_part(t, z, t, b).start()
+        vn[2 * z + lax.div(b, 2), rows(lax.rem(b, 2), 128), :] = v4[z, b]
+
+    with scope("values3"):
+        lax.fori_loop(0, 3, lambda n, c: (values(lax.rem(y + n + lax.div(n, 2), 4)), c)[1], 0)
     with scope("xfar"):
         xring.far()
-
-    def v_part(zz, src, to):
-        return remote(v4.at[to], vn.at[pl.ds(2 * src, 2)], vs.at[0], vr.at[src], zz * 4 + y, dp)
-
-    with scope("values"):
-        for n in (0, 1):
-            v = nn(xr[...].reshape(512, 2048), wq[:, :, :, n * 256:(n + 1) * 256].reshape(2048, 256)).astype(BF)
-            for m in (0, 1):
-                t = 2 * n + m
-                v4[t] = v[:, m * 128:(m + 1) * 128].reshape(2, B, 128)
-
-                @pl.when(t != z)
-                def _():
-                    v_part(t, z, t).start()
-        vn[pl.ds(2 * z, 2)] = v4[z]
+    with scope("values1"):
+        values(lax.rem(y + 2, 4))
+    with scope("columns"):
+        all_of(xc.at[0, pl.ds(0, 3)], zr)
+    cring.start()
 
     def mixed(r):
         def one(e, c):
@@ -349,17 +351,21 @@
             return c
         lax.fori_loop(0, 2, one, 0)
 
+    def all_v(t):
+        ref = vn.at[pl.ds(2 * t, 2)]
+        pltpu.make_async_copy(ref, ref, vr.at[t]).wait()
+
     with scope("mix0"):
         mixed(z)
     for d in (1, 3):
         t = lax.rem(z + d, 4)
         with scope("v%d" % d):
-            v_part(t, t, z).wait_recv()
+            all_v(t)
         with scope("mix%d" % d):
             mixed(t)
     t = lax.rem(z + 2, 4)
     with scope("v2"):
-        v_part(t, t, z).wait_recv()
+        all_v(t)
     with scope("mix2"):
         mixed(t)
     with scope("cot"):
@@ -401,18 +407,20 @@
     def gw_part(d, src, to, h):
         return remote(gwp.at[h, to], gwin.at[h, src], es.at[0], er.at[0], sp, d)
 
-    def send_head(o, weights):
+    def send_dv(o):
         h = lax.rem(z + o, 4)
-        if weights:
-            for n in range(4):
-                gwp[h, :, n] = gwt[h, :, n * 128:(n + 1) * 128].T.astype(BF).reshape(8, 16, 128)
-            dp_peers(lambda d: gw_part(d, dp, d, h).start())
-        else:
-            y_peers(lambda t: dv_part(t, y, t, h).start())
+        y_peers(lambda t: dv_part(t, y, t, h).start())
+
+    def send_weights(o):
+        h = lax.rem(z + o, 4)
+        g = sum(nn(dvg[h, 2 * b:2 * b + 2].reshape(512, 128).T, xc[:, b].reshape(512, 512)) for b in range(4))
+        for n in range(4):
+            gwp[h, :, n] = g[:, n * 128:(n + 1) * 128].T.astype(BF).reshape(8, 16, 128)
+        dp_peers(lambda d: gw_part(d, dp, d, h).start())
 
     def dv_ring(j):
         return Ring(lambda i, part: dvg.at[i, j] if part is None else dvg.at[i, j, pl.ds(128 * part, 128)],
-                    gs.at[0], lambda n: gr.at[j, n], z, along_z)
+                    gs.at[0], lambda n: gr.at[j, n] if n < 2 else gf.at[n - 2], z, along_z)
 
     def main(n, c):
         j = NB - 1 - n
@@ -447,7 +455,7 @@
         return c
     with scope("main"):
         lax.fori_loop(0, NB, main, 0)
-    send_head(0, False)
+    send_dv(0)
     save_k = pltpu.make_async_copy(gkb, gk_h, save.at[0])
     save_k.start()
 
@@ -458,51 +466,17 @@
         lax.fori_loop(0, NB, fin, 0)
     save_q = pltpu.make_async_copy(gqb, gq_h, save.at[1])
     save_q.start()
-    gwt[...] = jnp.zeros_like(gwt)
-
-    def weight_part(h, j):
-        jz, jy = lax.div(j, 2), lax.rem(j, 2)
-        cols = xc[pl.ds(2 * jy, 2), jz].reshape(B, 512)
-        gwt[h] += nn(dvg[h, j].T, cols)
-
-    def pieces(lo, hi, offsets):
-        def one(j, c):
-            for o in offsets:
-                weight_part(lax.rem(z + o, 4), j)
-            return c
-        lax.fori_loop(lo, hi, one, 0)
-
     with scope("near3"):
         dv_ring(3).near()
     with scope("cfar"):
         cring.full()
         cring.far()
-    with scope("pieces0"):
-        pieces(0, 8, (0,))
-        send_head(0, True)
-    with scope("near2"):
+    with scope("near21"):
         dv_ring(2).near()
+    with scope("weights0"):
+        send_weights(0)
     with scope("near1"):
         dv_ring(1).near()
-
-    def neighbours(lo, hi):
-        def one(n, c):
-            j = hi - 1 - n
-            dv_ring(j).full()
-            weight_part(lax.rem(z + 1, 4), j)
-            weight_part(lax.rem(z + 3, 4), j)
-            return c
-        lax.fori_loop(0, hi - lo, one, 0)
-    with scope("pieces13"):
-        neighbours(2, 8)
-    with scope("near0"):
-        dv_ring(0).near()
-    with scope("pieces01"):
-        neighbours(0, 2)
-    for o in (1, 3):
-        send_head(o, False)
-    for o in (1, 3):
-        send_head(o, True)
 
     def gather(o):
         h = lax.rem(z + o, 4)
@@ -515,15 +489,23 @@
         h = lax.rem(z + o, 4)
         return nt(dvrow[h], w[pl.ds(2 * n, 2), :, :, lanes(h, 512)].reshape(B, 512))
 
+    with scope("near0"):
+        dv_ring(0).near()
+    with scope("full"):
+        pltpu.make_async_copy(dvg.at[0], dvg.at[0], gf.at[0]).wait()
+    for o in (1, 3):
+        send_dv(o)
     with scope("wrowfar"):
         wrow.far()
         other(w, wrow, 2, wds, wdr).start()
+    with scope("weights13"):
+        for o in (1, 3):
+            send_weights(o)
     with scope("far"):
-        lax.fori_loop(0, NB, lambda n, c: (dv_ring(7 - n).far(), c)[1], 0)
-    send_head(2, False)
+        pltpu.make_async_copy(dvg.at[0], dvg.at[0], gf.at[1]).wait()
+    send_dv(2)
     with scope("distant"):
-        pieces(0, 8, (2,))
-    send_head(2, True)
+        send_weights(2)
     dp_peers(lambda d: gl_part(d, dp, d).start())
     glin[dp] = glb[...]
     for h in range(4):
@@ -626,13 +608,13 @@
         scratch_shapes=[
             V((4, 128, 2048), BF), V((4, 4, 128, 512), BF), V((16, 8, 16, 2048), BF), V((4, 16, 512), BF), V((16, 8, 16, 512), BF),
             V((L, 128), BF), V((L, 128), BF), V((L, 128), BF),
-            V((NB, B, 128), BF), V((NB, B, 128), BF), V((NB, 128, B), BF), V((NB, 128, B), BF), V((NB, B, 128), BF), V((4, 2, B, 128), BF),
+            V((NB, B, 128), BF), V((NB, B, 128), BF), V((NB, 128, B), BF), V((NB, 128, B), BF), V((NB, B, 128), BF), V((4, 4, 128, 128), BF),
             V((NB, B, B), F32), V((NB, B, B), F32), V(tiles, BF), V(tiles, BF), V(tiles, BF),
             V((NB, 128, B), BF), V((NB, B, 128), BF), V((NB, 8, B), F32), V((NB, 128, B), F32), V((NB, 128, B), F32), V((NB, 128, B), F32),
-            V((4, NB, B, 128), BF), V((4, 4, 128, 128), BF), V((4, 128, 512), BF), V((128, 2048), F32), V((4, 128, 512), F32), V((4, 8, 4, 16, 128), BF), V((4, 8, 4, 16, 128), BF),
+            V((4, NB, B, 128), BF), V((4, 4, 128, 128), BF), V((4, 128, 512), BF), V((128, 2048), F32), V((4, 8, 4, 16, 128), BF), V((4, 8, 4, 16, 128), BF),
             V((4, 4, 16, 128), BF), V((4, 4, 16, 128), BF), V((L, 128), BF), V((L, 128), BF), V((128, 2048), BF), V((16, 2048), F32),
             V((8, 128), F32), V((8, 8, 128), F32), pltpu.SMEM((1,), F32),
-            dma(6), dma(1), dma(5), dma(1), dma(4), dma(1), dma(4), dma(1), dma(1), dma(2), dma(2, 4), dma(1), dma(4), dma(1), dma(4), dma(1), dma(1), dma(1), dma(1), dma(1), dma(4), dma(1), dma(8, 4), dma(1), dma(4), dma(1), dma(1), dma(1), dma(1), dma(1), dma(1), dma(1), dma(1), dma(1), dma(1)],
+            dma(6), dma(1), dma(5), dma(1), dma(4), dma(1), dma(4), dma(1), dma(1), dma(2), dma(2, 4), dma(1), dma(4), dma(1), dma(4), dma(1), dma(1), dma(1), dma(1), dma(1), dma(4), dma(1), dma(8, 2), dma(1), dma(4), dma(1), dma(1), dma(1), dma(1), dma(1), dma(1), dma(1), dma(1), dma(1), dma(1), dma(2)],
         compiler_params=pltpu.CompilerParams(vmem_limit_bytes=60 * 1024 * 1024, collective_id=0, has_side_effects=True),
         name="whole")(lambdas, tokens[0], cotangent[0], value_weight, query_heads.reshape(L, 128), key_heads.reshape(L, 128))
     gq, gk, gt, gw, gl = pl.pallas_call(

time: 84.4 us -> 83.5 us (0.989)
  Pallas kernels: 82.9 us -> 82 us
    pallas_call x1, Pallas kernels: 80.1 us -> 79.2 us  [body(): pl.pallas_call(kernel, out_shape=(S((L, 128), BF), S((L, 128), BF), S((12...]
where the time goes in v5:
time: 83.5 us; the launch traced here: 83.3 us
  Pallas kernels  82 us (98%)
  between operations  1.29 us (2%)
    pallas_call x1, Pallas kernels, body(): pl.pallas_call(kernel, out_shape=(S((L, 128), BF), S((L, 128), BF), S((12...  79.2 us
    pallas_call x1, Pallas kernels, body(): pl.pallas_call(hand_out, out_shape=(S((L, 128), BF), S((L, 128), BF), S((...  2.81 us

profile of v5, /device:TPU:1, one launch (start us, length us, event | category | flops | bytes accessed | tf_op | source)
XLA Modules:
  0.0 83.3 jit_solution(17908526777783305870)
XLA Ops:
  1.3 79.2 %whole.1 = (bf16[2048,128]{1,0:T(8,128)(2,1)}, bf16[2048,128]{1,0:T(8,128)(2,1)}, bf16[128,2048]{1,0:T(8,128)(2,1)}, f32[16,2048]{1,0:T(8,128)}, f32[8,128]{1,0:T(8,128)}) custom-call(f32[1]{0:T(128)S(6)} %copy.11.lam_h, bf16[128,2048]{1,0:T(8,128)(2,1)} %bitcast.7, bf16[128,2048]{1,0:T(8,128)(2,1)} %bitcast.8, bf16[16,2048]{1,0:T(8,128)(2,1)} %w_h.1, ...), custom_call_target="tpu_custom_call" | custom-call | tf_op jit(solution)/shard_map/whole/pallas_call | solution.py:604
  80.5 2.8 %hand_out.1 = (bf16[2048,128]{1,0:T(8,128)(2,1)}, bf16[2048,128]{1,0:T(8,128)(2,1)}, bf16[128,2048]{1,0:T(8,128)(2,1)}, f32[16,2048]{1,0:T(8,128)}, f32[1]{0:T(128)}) custom-call(bf16[2048,128]{1,0:T(8,128)(2,1)} %get-tuple-element.15.refs_0_, bf16[2048,128]{1,0:T(8,128)(2,1)} %get-tuple-element.16.refs_1_, bf16[128,2048]{1,0:T(8,128)(2,1)} %get-tuple-element.17.refs_2_, ...), custom_call_target="tpu_custom_call" | custom-call | tf_op jit(solution)/shard_map/hand_out/pallas_call | solution.py:620

commit v6 on v5

--- a/solution.py
+++ b/solution.py
@@ -294,7 +294,7 @@
     with scope("qnear"):
         qrow.near()
         qrow.full()
-        for o in (-1, 1):
+        for o in (1, -1):
             other(wq, qrow, o, qds, qdr).start()
     with scope("wznear"):
         wz.near()
@@ -307,7 +307,6 @@
         wz.full()
         wz.far()
     wrow.start()
-    other(w, wrow, 0, wds, wdr).start()
     with scope("qfar"):
         qrow.far()
         other(wq, qrow, 2, qds, qdr).start()
@@ -368,6 +367,7 @@
         all_v(t)
     with scope("mix2"):
         mixed(t)
+    other(w, wrow, 0, wds, wdr).start()
     with scope("cot"):
         loads[4].wait()
         all_of(cota.at[pl.ds(0, 1920)], cr)
@@ -520,7 +520,7 @@
         gta[:, rows(n)] = times_rows(n, 0) + times_rows(n, 1) + times_rows(n, 3)
         return c
     with scope("tgrada"):
-        lax.fori_loop(0, NB, most, 0)
+        lax.fori_loop(0, 6, most, 0)
     with scope("gwwait"):
         all_of(gwin.at[:, pl.ds(0, 7)], er)
     for h in range(4):
@@ -540,6 +540,8 @@
     delta[0] = jnp.concatenate([tot, tot], axis=1)
     save_l = pltpu.make_async_copy(delta.at[0, :, pl.ds(0, 128)], gl_h, save.at[3])
     save_l.start()
+    with scope("tgradc"):
+        lax.fori_loop(6, NB, most, 0)
     with scope("dvwait"):
         gather(2)
 
@@ -580,16 +582,14 @@
 
 
 def hand_out(*refs):
-    came, outs, held, (got, put) = refs[:5], refs[5:10], refs[10:15], refs[15:]
-    loads = [pltpu.make_async_copy(came[n], held[n], got.at[n]) for n in range(5)]
-    saves = [pltpu.make_async_copy(held[n], outs[n], put.at[n]) for n in range(4)]
-    for a in loads:
+    came, outs, (held, got, put) = refs[:5], refs[5:10], refs[10:]
+    saves = [pltpu.make_async_copy(came[n], outs[n], put.at[n]) for n in range(4)]
+    scalar = pltpu.make_async_copy(came[4], held, got.at[0])
+    scalar.start()
+    for a in saves:
         a.start()
-    for n in range(4):
-        loads[n].wait()
-        saves[n].start()
-    loads[4].wait()
-    outs[4][0] = held[4][0, 0]
+    scalar.wait()
+    outs[4][0] = held[0, 0]
     for a in saves:
         a.wait()
 
@@ -615,14 +615,14 @@
             V((4, 4, 16, 128), BF), V((4, 4, 16, 128), BF), V((L, 128), BF), V((L, 128), BF), V((128, 2048), BF), V((16, 2048), F32),
             V((8, 128), F32), V((8, 8, 128), F32), pltpu.SMEM((1,), F32),
             dma(6), dma(1), dma(5), dma(1), dma(4), dma(1), dma(4), dma(1), dma(1), dma(2), dma(2, 4), dma(1), dma(4), dma(1), dma(4), dma(1), dma(1), dma(1), dma(1), dma(1), dma(4), dma(1), dma(8, 2), dma(1), dma(4), dma(1), dma(1), dma(1), dma(1), dma(1), dma(1), dma(1), dma(1), dma(1), dma(1), dma(2)],
-        compiler_params=pltpu.CompilerParams(vmem_limit_bytes=60 * 1024 * 1024, collective_id=0, has_side_effects=True),
+        compiler_params=pltpu.CompilerParams(vmem_limit_bytes=53000 * 1024, collective_id=0, has_side_effects=True),
         name="whole")(lambdas, tokens[0], cotangent[0], value_weight, query_heads.reshape(L, 128), key_heads.reshape(L, 128))
     gq, gk, gt, gw, gl = pl.pallas_call(
         hand_out,
         out_shape=(S((L, 128), BF), S((L, 128), BF), S((128, 2048), BF), S((16, 2048), F32), S((1,), F32)),
-        in_specs=[hbm] * 5, out_specs=[hbm] * 4 + [smem],
-        scratch_shapes=[V((L, 128), BF), V((L, 128), BF), V((128, 2048), BF), V((16, 2048), F32), pltpu.SMEM((8, 128), F32), dma(5), dma(4)],
-        compiler_params=pltpu.CompilerParams(vmem_limit_bytes=60 * 1024 * 1024),
+        in_specs=[anywhere] * 5, out_specs=[hbm] * 4 + [smem],
+        scratch_shapes=[pltpu.SMEM((8, 128), F32), dma(1), dma(4)],
+        compiler_params=pltpu.CompilerParams(vmem_limit_bytes=8 * 1024 * 1024),
         name="hand_out")(gq, gk, gt, gw, gl)
     return gq.reshape(query_heads.shape), gk.reshape(key_heads.shape), gt[None], gw, gl
 

time: 83.5 us -> 82.3 us (0.986)
  Pallas kernels: 82 us -> 80 us
    pallas_call x1, Pallas kernels: 2.81 us -> 1.74 us  [body(): pl.pallas_call(hand_out, out_shape=(S((L, 128), BF), S((L, 128), BF), S((...]
    pallas_call x1, Pallas kernels: 79.2 us -> 78.2 us  [body(): pl.pallas_call(kernel, out_shape=(S((L, 128), BF), S((L, 128), BF), S((12...]
where the time goes in v6:
time: 82.3 us; the launch traced here: 82.1 us
  Pallas kernels  80 us (97%)
  between operations  1.3 us (2%)
  local copies, waits for them, and re-layouts  0.83 us (1%)
    pallas_call x1, Pallas kernels, body(): pl.pallas_call(kernel, out_shape=(S((L, 128), BF), S((L, 128), BF), S((12...  78.2 us
    pallas_call x1, Pallas kernels, body(): pl.pallas_call(hand_out, out_shape=(S((L, 128), BF), S((L, 128), BF), S((...  1.74 us

profile of v6, /device:TPU:1, one launch (start us, length us, event | category | flops | bytes accessed | tf_op | source)
XLA Modules:
  0.0 82.1 jit_solution(13657484454388623924)
XLA Ops:
  1.3 0.0 copy-start
  1.3 0.8 %copy-done = bf16[16,2048]{1,0:T(8,128)(2,1)S(1)} copy-done((bf16[16,2048]{1,0:T(8,128)(2,1)S(1)}, bf16[16,2048]{1,0:T(8,128)(2,1)}, u32[]{:S(2)}) %copy-start) | copy-done | bytes 65560
  2.1 78.2 %whole.1 = (bf16[2048,128]{1,0:T(8,128)(2,1)S(1)}, bf16[2048,128]{1,0:T(8,128)(2,1)S(1)}, bf16[128,2048]{1,0:T(8,128)(2,1)S(1)}, f32[16,2048]{1,0:T(8,128)S(1)}, f32[8,128]{1,0:T(8,128)S(1)}) custom-call(f32[1]{0:T(128)S(6)} %copy.11.lam_h, bf16[128,2048]{1,0:T(8,128)(2,1)} %bitcast.7, bf16[128,2048]{1,0:T(8,128)(2,1)} %bitcast.8, ...), custom_call_target="tpu_custom_call" | custom-call | tf_op jit(solution)/shard_map/whole/pallas_call | solution.py:604
  80.4 1.7 %hand_out.1 = (bf16[2048,128]{1,0:T(8,128)(2,1)}, bf16[2048,128]{1,0:T(8,128)(2,1)}, bf16[128,2048]{1,0:T(8,128)(2,1)}, f32[16,2048]{1,0:T(8,128)}, f32[1]{0:T(128)}) custom-call(bf16[2048,128]{1,0:T(8,128)(2,1)S(1)} %get-tuple-element.15.refs_0_, bf16[2048,128]{1,0:T(8,128)(2,1)S(1)} %get-tuple-element.16.refs_1_, ...), custom_call_target="tpu_custom_call" | custom-call | tf_op jit(solution)/shard_map/hand_out/pallas_call | solution.py:620
Async XLA Ops:
  1.3 0.8 %copy-start = (bf16[16,2048]{1,0:T(8,128)(2,1)S(1)}, bf16[16,2048]{1,0:T(8,128)(2,1)}, u32[]{:S(2)}) copy-start(bf16[16,2048]{1,0:T(8,128)(2,1)} %w_h.1) | copy-start | bytes 196612

commit v7 on v6

--- a/solution.py
+++ b/solution.py
@@ -148,25 +148,24 @@
 
     def start(self):
         self.copy(0, 0, 1, 0).start()
-        self.copy(0, 1, -1, 1).start()
-        self.copy(0, 1, 1, 2).start()
-        self.copy(0, 0, -1, 2).start()
+        self.copy(0, 1, -1, 0).start()
+        self.copy(0, 1, 1, 1).start()
+        self.copy(0, 0, -1, 1).start()
 
     def near(self):
-        self.copy(-1, 0, 1, 0).wait_recv()
-        self.copy(-1, 0, 1, 3).start()
-        self.copy(1, 1, -1, 1).wait_recv()
-        self.copy(1, 1, -1, 3).start()
+        self.both(1, 0)
+        self.copy(-1, 0, 1, 2).start()
+        self.copy(1, 1, -1, 2).start()
 
     def both(self, o, sem):
         ref = self.at(self.index(o), None)
         pltpu.make_async_copy(ref, ref, self.rs(sem)).wait()
 
     def full(self):
-        self.both(1, 2)
+        self.both(1, 1)
 
     def far(self):
-        self.both(2, 3)
+        self.both(2, 2)
 
 
 def kernel(lam_h, tok_h, cot_h, w_h, q_h, k_h, gq_h, gk_h, gt_h, gw_h, gl_h,
@@ -420,7 +419,7 @@
 
     def dv_ring(j):
         return Ring(lambda i, part: dvg.at[i, j] if part is None else dvg.at[i, j, pl.ds(128 * part, 128)],
-                    gs.at[0], lambda n: gr.at[j, n] if n < 2 else gf.at[n - 2], z, along_z)
+                    gs.at[0], lambda n: gr.at[j] if n < 1 else gf.at[n - 1], z, along_z)
 
     def main(n, c):
         j = NB - 1 - n
@@ -614,7 +613,7 @@
             V((4, NB, B, 128), BF), V((4, 4, 128, 128), BF), V((4, 128, 512), BF), V((128, 2048), F32), V((4, 8, 4, 16, 128), BF), V((4, 8, 4, 16, 128), BF),
             V((4, 4, 16, 128), BF), V((4, 4, 16, 128), BF), V((L, 128), BF), V((L, 128), BF), V((128, 2048), BF), V((16, 2048), F32),
             V((8, 128), F32), V((8, 8, 128), F32), pltpu.SMEM((1,), F32),
-            dma(6), dma(1), dma(5), dma(1), dma(4), dma(1), dma(4), dma(1), dma(1), dma(2), dma(2, 4), dma(1), dma(4), dma(1), dma(4), dma(1), dma(1), dma(1), dma(1), dma(1), dma(4), dma(1), dma(8, 2), dma(1), dma(4), dma(1), dma(1), dma(1), dma(1), dma(1), dma(1), dma(1), dma(1), dma(1), dma(1), dma(2)],
+            dma(6), dma(1), dma(5), dma(1), dma(3), dma(1), dma(3), dma(1), dma(1), dma(2), dma(2, 3), dma(1), dma(3), dma(1), dma(3), dma(1), dma(1), dma(1), dma(1), dma(1), dma(4), dma(1), dma(8), dma(1), dma(4), dma(1), dma(1), dma(1), dma(1), dma(1), dma(1), dma(1), dma(1), dma(1), dma(1), dma(2)],
         compiler_params=pltpu.CompilerParams(vmem_limit_bytes=53000 * 1024, collective_id=0, has_side_effects=True),
         name="whole")(lambdas, tokens[0], cotangent[0], value_weight, query_heads.reshape(L, 128), key_heads.reshape(L, 128))
     gq, gk, gt, gw, gl = pl.pallas_call(

time: 82.3 us -> 82 us (level)
  no operation moved by 1% of the time
where the time goes in v7:
time: 82 us; the launch traced here: 81.8 us
  Pallas kernels  79.7 us (97%)
  between operations  1.3 us (2%)
  local copies, waits for them, and re-layouts  0.83 us (1%)
    pallas_call x1, Pallas kernels, body(): pl.pallas_call(kernel, out_shape=(S((L, 128), BF), S((L, 128), BF), S((12...  78 us
    pallas_call x1, Pallas kernels, body(): pl.pallas_call(hand_out, out_shape=(S((L, 128), BF), S((L, 128), BF), S((...  1.74 us

profile of v7, /device:TPU:1, one launch (start us, length us, event | category | flops | bytes accessed | tf_op | source)
XLA Modules:
  0.0 81.8 jit_solution(13008182988909323352)
XLA Ops:
  1.3 0.0 copy-start
  1.3 0.8 %copy-done = bf16[16,2048]{1,0:T(8,128)(2,1)S(1)} copy-done((bf16[16,2048]{1,0:T(8,128)(2,1)S(1)}, bf16[16,2048]{1,0:T(8,128)(2,1)}, u32[]{:S(2)}) %copy-start) | copy-done | bytes 65560
  2.1 78.0 %whole.1 = (bf16[2048,128]{1,0:T(8,128)(2,1)S(1)}, bf16[2048,128]{1,0:T(8,128)(2,1)S(1)}, bf16[128,2048]{1,0:T(8,128)(2,1)S(1)}, f32[16,2048]{1,0:T(8,128)S(1)}, f32[8,128]{1,0:T(8,128)S(1)}) custom-call(f32[1]{0:T(128)S(6)} %copy.11.lam_h, bf16[128,2048]{1,0:T(8,128)(2,1)} %bitcast.7, bf16[128,2048]{1,0:T(8,128)(2,1)} %bitcast.8, ...), custom_call_target="tpu_custom_call" | custom-call | tf_op jit(solution)/shard_map/whole/pallas_call | solution.py:603
  80.1 1.7 %hand_out.1 = (bf16[2048,128]{1,0:T(8,128)(2,1)}, bf16[2048,128]{1,0:T(8,128)(2,1)}, bf16[128,2048]{1,0:T(8,128)(2,1)}, f32[16,2048]{1,0:T(8,128)}, f32[1]{0:T(128)}) custom-call(bf16[2048,128]{1,0:T(8,128)(2,1)S(1)} %get-tuple-element.15.refs_0_, bf16[2048,128]{1,0:T(8,128)(2,1)S(1)} %get-tuple-element.16.refs_1_, ...), custom_call_target="tpu_custom_call" | custom-call | tf_op jit(solution)/shard_map/hand_out/pallas_call | solution.py:619
Async XLA Ops:
  1.3 0.8 %copy-start = (bf16[16,2048]{1,0:T(8,128)(2,1)S(1)}, bf16[16,2048]{1,0:T(8,128)(2,1)}, u32[]{:S(2)}) copy-start(bf16[16,2048]{1,0:T(8,128)(2,1)} %w_h.1) | copy-start | bytes 196612
